TPU v7x, 128 devices: a whole 4x4x4 slice. The times are simulated.
128 devices in a mesh: sp: 64 (over z, y, x), tp: 2 (over core).
Axes of the slice: x: 4, y: 4, z: 4, core: 2. Of those that a mesh axis runs over, the one named last changes fastest.
Arguments:
- mid_stream: bfloat16 [20480, 2048], P('sp', 'tp'), may hold values from -6 to 6
- layer_cot: bfloat16 [20480, 2048], P('sp', 'tp'), may hold values from -16 to 16
- ffn_gain: bfloat16 [2048], P('tp'), may hold values from 0.099609375 to 1.8984375
- expert_ids: int32 [20480, 2], P('sp'), may hold values from 0 to 63, all different within a row; in each aligned block of 320 rows (0 to 319, 320 to 639, ...) at most 20 rows name the same one
- group_prob: float32 [20480], P('sp'), may hold values from 0.25 to 1
- first_share: float32 [20480], P('sp'), may hold values from 0.5 to 0.95
- expert_gate: bfloat16 [64, 2048, 1024], P('sp', None, 'tp'), may hold values from -0.125 to 0.125
- expert_up: bfloat16 [64, 2048, 1024], P('sp', None, 'tp'), may hold values from -0.125 to 0.125
- expert_down: bfloat16 [64, 1024, 2048], P('sp', 'tp'), may hold values from -0.1875 to 0.1875
- out_weight: bfloat16 [2048, 1024], P(None, 'tp'), may hold values from -0.1875 to 0.1875
- conv_gain: bfloat16 [1024], P('tp'), may hold values from 0.099609375 to 1.8984375
- b_gate: bfloat16 [20480, 1024], P('sp', 'tp'), may hold values from -6 to 6
- c_gate: bfloat16 [20480, 1024], P('sp', 'tp'), may hold values from -6 to 6
- conv_in: bfloat16 [20480, 1024], P('sp', 'tp'), may hold values from -6 to 6
- conv_out: bfloat16 [20480, 1024], P('sp', 'tp'), may hold values from -6 to 6
- conv_taps: bfloat16 [3, 1024], P(None, 'tp'), may hold values from -3.5 to 3.5
Outputs:
- grad_gate: float32 [64, 2048, 1024], P('sp', None, 'tp')
- grad_up: float32 [64, 2048, 1024], P('sp', None, 'tp')
- grad_down: float32 [64, 1024, 2048], P('sp', 'tp')
- grad_out_weight: float32 [2048, 1024], P('sp', 'tp')
- mid_grad: bfloat16 [20480, 2048], P('sp', 'tp')
- grad_b: bfloat16 [20480, 1024], P('sp', 'tp')
- grad_c: bfloat16 [20480, 1024], P('sp', 'tp')
- grad_conv_in: bfloat16 [20480, 1024], P('sp', 'tp')
Inputs may be any that keep to these rules, and one draw needn't show every extreme that they name: `expert_ids`: each row names 2 different experts. Among the rows of one device no expert is named more than 20 times, a bound that some block reaches.
All inputs are finite; a program needn't handle non-finite values.
Results may differ from a plain program's by a relative error of at most 0.0067.
Values may be sent and summed in bfloat16 or wider, within the bound.
A program may use at most 128 MiB of HBM per device.

v0:
```python
import functools

import jax
import jax.numpy as jnp
from jax import lax
from jax.experimental import pallas as pl
from jax.experimental.pallas import tpu as pltpu
from jax.sharding import PartitionSpec as P

D = 2048
HALF = 1024
GROUP = 64
TOK = 320
FF = 512
NDEV = 64
ROWS = 1280
CH = 256
epsilon = 1e-06

F32 = jnp.float32
BF16 = jnp.bfloat16
MESH = pl.DeviceIdType.MESH
VM = pl.BlockSpec(memory_space=pltpu.VMEM)
ANY = pl.BlockSpec(memory_space=pl.ANY)


def mm(a, b):
    return jnp.dot(a, b, preferred_element_type=F32)


def mm_nt(a, b):
    return lax.dot_general(a, b, (((1,), (1,)), ((), ())), preferred_element_type=F32)


def mm_tn(a, b):
    return lax.dot_general(a, b, (((0,), (0,)), ((), ())), preferred_element_type=F32)


def iota(shape, dim):
    return lax.broadcasted_iota(jnp.int32, shape, dim)


def ind(mask):
    return jnp.where(mask, 1.0, 0.0)


def greet(other):
    barrier = pltpu.get_barrier_semaphore()
    pl.semaphore_signal(barrier, inc=1, device_id=other, device_id_type=MESH)
    pl.semaphore_wait(barrier, 1)


def lane_slots(ids, ids_t):
    earlier = iota((TOK, TOK), 0) < iota((TOK, TOK), 1)
    out = []
    for c in range(2):
        mine = ids_t[c : c + 1, :]
        same = ind(earlier & (ids[:, 0:1] == mine)) + ind(earlier & (ids[:, 1:2] == mine))
        rank = jnp.sum(same, axis=0, keepdims=True).astype(jnp.int32)
        out.append(mine * 32 + rank)
    return out


def row_slots(ids, ids_t):
    earlier = iota((TOK, TOK), 1) < iota((TOK, TOK), 0)
    out = []
    for c in range(2):
        mine = ids[:, c : c + 1]
        same = ind(earlier & (ids_t[0:1, :] == mine)) + ind(earlier & (ids_t[1:2, :] == mine))
        rank = jnp.sum(same, axis=1, keepdims=True).astype(jnp.int32)
        out.append(mine * 32 + rank)
    return out


def prep_kernel(
    mid, cot, gain, ids, ids_t, prob, share, packed, inv_out, sq_mine, sq_other, normed, send, recv
):
    sp, tp = lax.axis_index("sp"), lax.axis_index("tp")
    other = (sp, 1 - tp)
    greet(other)
    m32 = mid[...].astype(F32)
    sq = jnp.sum(m32 * m32, axis=1, keepdims=True)
    sq_mine[...] = jnp.broadcast_to(sq, (TOK, 128))
    copy = pltpu.make_async_remote_copy(
        sq_mine, sq_other, send.at[0], recv.at[0], device_id=other, device_id_type=MESH
    )
    copy.start()
    slot0, slot1 = lane_slots(ids[...], ids_t[...])
    s0 = prob[...] * share[...]
    s1 = prob[...] * (1.0 - share[...])
    copy.wait()
    total = sq + sq_other[:, 0:1]
    inv = lax.rsqrt(total / D + epsilon)
    inv_out[...] = jnp.broadcast_to(inv, (TOK, 128))
    normed[...] = (m32 * inv * gain[...].astype(F32)).astype(BF16)

    def block(i, carry):
        e0 = i * 16
        r = iota((CH, 1), 0)
        code = (e0 + r // 16) * 32 + r % 16
        hit0 = code == slot0
        hit1 = code == slot1
        pick = ind(hit0 | hit1).astype(BF16)
        weight = jnp.sum(jnp.where(hit0, s0, 0.0) + jnp.where(hit1, s1, 0.0), axis=1, keepdims=True)
        tok = mm(pick, normed[...]).astype(BF16)
        ct = (mm(pick, cot[...]) * weight).astype(BF16)
        dst = pl.ds(e0, 16)
        packed[dst, 0:16, :] = tok[:, :512].reshape(16, 16, 512)
        packed[dst, 16:32, :] = tok[:, 512:].reshape(16, 16, 512)
        packed[dst, 32:48, :] = ct[:, :512].reshape(16, 16, 512)
        packed[dst, 48:64, :] = ct[:, 512:].reshape(16, 16, 512)
        part = (r // 4) % 4
        code = (e0 + r // 16) * 32 + 16 + r % 4
        hit0 = code == slot0
        hit1 = code == slot1
        hit = hit0 | hit1
        weight = jnp.sum(jnp.where(hit0, s0, 0.0) + jnp.where(hit1, s1, 0.0), axis=1, keepdims=True)
        acc = mm(ind(hit & (part == 0)).astype(BF16), normed[:, :512])
        acc += mm(ind(hit & (part == 1)).astype(BF16), normed[:, 512:])
        acc += mm(ind(hit & (part == 2)).astype(BF16), cot[:, :512])
        acc += mm(ind(hit & (part == 3)).astype(BF16), cot[:, 512:])
        acc = acc * jnp.where(part >= 2, weight, 1.0)
        packed[dst, 64:80, :] = acc.astype(BF16).reshape(16, 16, 512)
        return carry

    lax.fori_loop(0, 4, block, 0)


def prep(mid, cot, gain, ids, ids_t, prob, share):
    return pl.pallas_call(
        prep_kernel,
        name="prep",
        out_shape=(
            jax.ShapeDtypeStruct((NDEV, 80, 512), BF16),
            jax.ShapeDtypeStruct((TOK, 128), F32),
        ),
        in_specs=[VM] * 7,
        out_specs=(VM, VM),
        scratch_shapes=[
            pltpu.VMEM((TOK, 128), F32),
            pltpu.VMEM((TOK, 128), F32),
            pltpu.VMEM((TOK, HALF), BF16),
            pltpu.SemaphoreType.DMA((1,)),
            pltpu.SemaphoreType.DMA((1,)),
        ],
        compiler_params=pltpu.CompilerParams(
            collective_id=1, has_side_effects=True, vmem_limit_bytes=40 * 2**20
        ),
        cost_estimate=pl.CostEstimate(
            flops=6 * 10**9, bytes_accessed=7 * 10**6, transcendentals=0
        ),
    )(mid, cot, gain, ids, ids_t, prob, share)


def expert_kernel(
    rin,
    wg,
    wu,
    wd,
    ret,
    tok_out,
    cot_out,
    hid_out,
    dg_out,
    du_out,
    tok,
    cots,
    acc_g,
    acc_u,
    acc_h,
    hid,
    dg,
    du,
    mine,
    theirs,
    got,
    tsend,
    trecv,
    csend,
    crecv,
    bsend,
    brecv,
    osem,
):
    sp, tp = lax.axis_index("sp"), lax.axis_index("tp")
    other = (sp, 1 - tp)
    own_cols = pl.ds(pl.multiple_of(tp * HALF, HALF), HALF)
    oth_cols = pl.ds(pl.multiple_of((1 - tp) * HALF, HALF), HALF)
    greet(other)

    def rows_of(i):
        return pl.ds(pl.multiple_of(i * CH, CH), CH)

    def swap(buf, half, i, send, recv):
        return pltpu.make_async_remote_copy(
            buf.at[half, rows_of(i)],
            buf.at[half, rows_of(i)],
            send.at[i],
            recv.at[i],
            device_id=other,
            device_id_type=MESH,
        )

    def gather_a(i, carry):
        src = pl.ds(i * 16, 16)
        rows = rows_of(i)
        tok[tp, rows, 0:512] = rin[src, 0:16, :].reshape(CH, 512)
        tok[tp, rows, 512:1024] = rin[src, 16:32, :].reshape(CH, 512)
        cots[tp, rows, 0:512] = rin[src, 32:48, :].reshape(CH, 512)
        cots[tp, rows, 512:1024] = rin[src, 48:64, :].reshape(CH, 512)
        swap(tok, tp, i, tsend, trecv).start()
        swap(cots, tp, i, csend, crecv).start()
        return carry

    lax.fori_loop(0, 4, gather_a, 0)

    def gather_b(i, carry):
        mixed = rin[pl.ds(i * 16, 16), 64:80, :].reshape(CH, 512)
        rows = pl.ds(pl.multiple_of(1024 + i * 64, 64), 64)
        r = iota((64, CH), 0)
        c = iota((64, CH), 1)
        want = (r // 4) * 16 + r % 4
        for part, (buf, lo) in enumerate(((tok, 0), (tok, 512), (cots, 0), (cots, 512))):
            move = ind(c == want + part * 4).astype(BF16)
            buf[tp, rows, lo : lo + 512] = mm(move, mixed).astype(BF16)
        return carry

    lax.fori_loop(0, 4, gather_b, 0)
    swap(tok, tp, 4, tsend, trecv).start()
    swap(cots, tp, 4, csend, crecv).start()

    def own_part(i, carry):
        rows = rows_of(i)
        x = tok[tp, rows, :]
        y = cots[tp, rows, :]
        acc_g[rows, :] = mm(x, wg[own_cols, :])
        acc_u[rows, :] = mm(x, wu[own_cols, :])
        acc_h[rows, :] = mm_nt(y, wd[:, own_cols])
        return carry

    lax.fori_loop(0, 5, own_part, 0)
    keep = [
        pltpu.make_async_copy(tok.at[tp], tok_out.at[:, own_cols], osem.at[0]),
        pltpu.make_async_copy(cots.at[tp], cot_out.at[:, own_cols], osem.at[1]),
    ]
    for k in keep:
        k.start()

    def back_copy(i):
        return pltpu.make_async_remote_copy(
            theirs.at[rows_of(i)],
            got.at[rows_of(i)],
            bsend.at[i],
            brecv.at[i],
            device_id=other,
            device_id_type=MESH,
        )

    def rest(i, carry):
        rows = rows_of(i)
        swap(tok, 1 - tp, i, tsend, trecv).wait_recv()
        swap(cots, 1 - tp, i, csend, crecv).wait_recv()
        x = tok[1 - tp, rows, :]
        y = cots[1 - tp, rows, :]
        pre_g = acc_g[rows, :] + mm(x, wg[oth_cols, :])
        pre_u = acc_u[rows, :] + mm(x, wu[oth_cols, :])
        d_h = acc_h[rows, :] + mm_nt(y, wd[:, oth_cols])
        sigma = jax.nn.sigmoid(pre_g)
        active = pre_g * sigma
        slope = sigma * (1.0 + pre_g * (1.0 - sigma))
        hid[rows, :] = (active * pre_u).astype(BF16)
        g = (d_h * pre_u * slope).astype(BF16)
        u = (d_h * active).astype(BF16)
        dg[rows, :] = g
        du[rows, :] = u
        theirs[rows, :] = (mm_nt(g, wg[oth_cols, :]) + mm_nt(u, wu[oth_cols, :])).astype(BF16)
        back_copy(i).start()
        mine[rows, :] = (mm_nt(g, wg[own_cols, :]) + mm_nt(u, wu[own_cols, :])).astype(BF16)
        return carry

    lax.fori_loop(0, 5, rest, 0)
    keep2 = [
        pltpu.make_async_copy(tok.at[1 - tp], tok_out.at[:, oth_cols], osem.at[2]),
        pltpu.make_async_copy(cots.at[1 - tp], cot_out.at[:, oth_cols], osem.at[3]),
        pltpu.make_async_copy(hid, hid_out, osem.at[4]),
        pltpu.make_async_copy(dg, dg_out, osem.at[5]),
        pltpu.make_async_copy(du, du_out, osem.at[6]),
    ]
    for k in keep2:
        k.start()

    def total(rows):
        return (mine[rows, :].astype(F32) + got[rows, :].astype(F32)).astype(BF16)

    def finish_a(i, carry):
        back_copy(i).wait_recv()
        s = total(rows_of(i))
        src = pl.ds(i * 16, 16)
        for q in range(4):
            ret[src, q * 16 : (q + 1) * 16, :] = s[:, q * 256 : (q + 1) * 256].reshape(16, 16, 256)
        return carry

    lax.fori_loop(0, 4, finish_a, 0)
    back_copy(4).wait_recv()

    def finish_b(i, carry):
        s = total(pl.ds(pl.multiple_of(1024 + i * 64, 64), 64))
        r = iota((CH, 64), 0)
        c = iota((CH, 64), 1)
        want = (r // 16) * 4 + r % 4
        part = (r // 4) % 4
        acc = jnp.zeros((CH, 256), F32)
        for q in range(4):
            move = ind((c == want) & (part == q)).astype(BF16)
            acc += mm(move, s[:, q * 256 : (q + 1) * 256])
        ret[pl.ds(i * 16, 16), 64:80, :] = acc.astype(BF16).reshape(16, 16, 256)
        return carry

    lax.fori_loop(0, 4, finish_b, 0)

    def drain(i, carry):
        swap(tok, tp, i, tsend, trecv).wait_send()
        swap(cots, tp, i, csend, crecv).wait_send()
        back_copy(i).wait_send()
        return carry

    lax.fori_loop(0, 5, drain, 0)
    for k in keep + keep2:
        k.wait()


def expert(rin, wg, wu, wd):
    return pl.pallas_call(
        expert_kernel,
        name="expert",
        out_shape=(
            jax.ShapeDtypeStruct((NDEV, 80, 256), BF16),
            jax.ShapeDtypeStruct((ROWS, D), BF16),
            jax.ShapeDtypeStruct((ROWS, D), BF16),
            jax.ShapeDtypeStruct((ROWS, FF), BF16),
            jax.ShapeDtypeStruct((ROWS, FF), BF16),
            jax.ShapeDtypeStruct((ROWS, FF), BF16),
        ),
        in_specs=[VM] * 4,
        out_specs=(VM, ANY, ANY, ANY, ANY, ANY),
        scratch_shapes=[
            pltpu.VMEM((2, ROWS, HALF), BF16),
            pltpu.VMEM((2, ROWS, HALF), BF16),
            pltpu.VMEM((ROWS, FF), F32),
            pltpu.VMEM((ROWS, FF), F32),
            pltpu.VMEM((ROWS, FF), F32),
            pltpu.VMEM((ROWS, FF), BF16),
            pltpu.VMEM((ROWS, FF), BF16),
            pltpu.VMEM((ROWS, FF), BF16),
            pltpu.VMEM((ROWS, HALF), BF16),
            pltpu.VMEM((ROWS, HALF), BF16),
            pltpu.VMEM((ROWS, HALF), BF16),
            pltpu.SemaphoreType.DMA((5,)),
            pltpu.SemaphoreType.DMA((5,)),
            pltpu.SemaphoreType.DMA((5,)),
            pltpu.SemaphoreType.DMA((5,)),
            pltpu.SemaphoreType.DMA((5,)),
            pltpu.SemaphoreType.DMA((5,)),
            pltpu.SemaphoreType.DMA((7,)),
        ],
        compiler_params=pltpu.CompilerParams(
            collective_id=2, has_side_effects=True, vmem_limit_bytes=58 * 2**20
        ),
        cost_estimate=pl.CostEstimate(
            flops=14 * 10**9, bytes_accessed=30 * 10**6, transcendentals=655360
        ),
    )(rin, wg, wu, wd)


def tail_kernel(
    back,
    mid,
    cot,
    gain,
    ids,
    ids_t,
    inv_in,
    bg,
    co,
    cgain,
    ow,
    gow,
    mgrad,
    gb,
    dco,
    in_mine,
    in_other,
    mg,
    send,
    recv,
):
    sp, tp = lax.axis_index("sp"), lax.axis_index("tp")
    other = (sp, 1 - tp)
    own_rows = pl.ds(pl.multiple_of(tp * HALF, HALF), HALF)
    oth_rows = pl.ds(pl.multiple_of((1 - tp) * HALF, HALF), HALF)
    greet(other)
    slot0, slot1 = row_slots(ids[...], ids_t[...])
    r = iota((1, HALF), 1)
    code = (r // 16) * 32 + r % 16
    pick_a = ind((code == slot0) | (code == slot1)).astype(BF16)
    code = (r // 16) * 32 + 16 + r % 4
    hit = (code == slot0) | (code == slot1)
    part = (r // 4) % 4
    mixed = back[:, 64:80, :].reshape(HALF, 256)
    pieces = []
    for q in range(4):
        d = mm(pick_a, back[:, q * 16 : (q + 1) * 16, :].reshape(HALF, 256))
        d += mm(ind(hit & (part == q)).astype(BF16), mixed)
        pieces.append(d)
    g_dn = jnp.concatenate(pieces, axis=1) * gain[...].astype(F32)
    m32 = mid[...].astype(F32)
    inner = jnp.sum(m32 * g_dn, axis=1, keepdims=True)
    in_mine[...] = jnp.broadcast_to(inner, (TOK, 128))
    copy = pltpu.make_async_remote_copy(
        in_mine, in_other, send.at[0], recv.at[0], device_id=other, device_id_type=MESH
    )
    copy.start()
    b32 = bg[...].astype(F32)
    y32 = co[...].astype(F32)
    cg = cgain[...].astype(F32)
    gated = b32 * y32
    same = ind(iota((512, 512), 0) // GROUP == iota((512, 512), 1) // GROUP)

    def group_mean(v):
        hi = v.astype(BF16)
        rest = v - hi.astype(F32)
        md = rest.astype(BF16)
        lo = (rest - md.astype(F32)).astype(BF16)
        ones = same.astype(BF16)
        return (mm(hi, ones) + mm(md, ones) + mm(lo, ones)) / GROUP

    rms = lax.rsqrt(group_mean(gated * gated) + epsilon)
    conv_normed = (gated * rms * cg).astype(BF16)
    copy.wait()
    inv = inv_in[:, 0:1]
    mean = (inner + in_other[:, 0:1]) / D
    total = cot[...].astype(F32) + inv * g_dn - m32 * (inv * inv * inv * mean)
    mgb = total.astype(BF16)
    mgrad[...] = mgb
    mg[tp] = mgb
    swap = pltpu.make_async_remote_copy(
        mg.at[tp], mg.at[tp], send.at[1], recv.at[1], device_id=other, device_id_type=MESH
    )
    swap.start()
    gow[own_rows, :] = mm_tn(mgb, conv_normed).astype(BF16)
    d_cn = mm(mgb, ow[own_rows, :])
    swap.wait()
    mo = mg[1 - tp]
    gow[oth_rows, :] = mm_tn(mo, conv_normed).astype(BF16)
    g_dc = cg * (d_cn + mm(mo, ow[oth_rows, :]))
    gmean = group_mean(gated * g_dc)
    d_gated = rms * g_dc - gated * (rms * rms * rms * gmean)
    gb[...] = (d_gated * y32).astype(BF16)
    dco[...] = d_gated * b32


def tail(*args):
    return pl.pallas_call(
        tail_kernel,
        name="tail",
        out_shape=(
            jax.ShapeDtypeStruct((D, 512), BF16),
            jax.ShapeDtypeStruct((TOK, HALF), BF16),
            jax.ShapeDtypeStruct((TOK, 512), BF16),
            jax.ShapeDtypeStruct((TOK, 512), F32),
        ),
        in_specs=[VM] * 11,
        out_specs=(VM,) * 4,
        scratch_shapes=[
            pltpu.VMEM((TOK, 128), F32),
            pltpu.VMEM((TOK, 128), F32),
            pltpu.VMEM((2, TOK, HALF), BF16),
            pltpu.SemaphoreType.DMA((2,)),
            pltpu.SemaphoreType.DMA((2,)),
        ],
        compiler_params=pltpu.CompilerParams(
            collective_id=3, has_side_effects=True, vmem_limit_bytes=40 * 2**20
        ),
        cost_estimate=pl.CostEstimate(
            flops=5 * 10**9, bytes_accessed=12 * 10**6, transcendentals=0
        ),
    )(*args)


def from_behind(block, axis, distance):
    devices = range(lax.axis_size(axis))
    route = [(i - distance, i) for i in devices if i - distance in devices]
    return lax.ppermute(block, axis, route)


def contract_rows(left, right):
    return lax.dot_general(
        left, right, (((0,), (0,)), ((), ())), preferred_element_type=jnp.float32
    )


def shards(
    mid_stream,
    layer_cot,
    ffn_gain,
    expert_ids,
    group_prob,
    first_share,
    expert_gate,
    expert_up,
    expert_down,
    out_weight,
    conv_gain,
    b_gate,
    c_gate,
    conv_in,
    conv_out,
    conv_taps,
):
    ids_t = expert_ids.T
    gain = ffn_gain.reshape(1, HALF)
    packed, inv = prep(
        mid_stream,
        layer_cot,
        gain,
        expert_ids,
        ids_t,
        group_prob.reshape(1, TOK),
        first_share.reshape(1, TOK),
    )
    arrived = lax.all_to_all(packed, "sp", split_axis=0, concat_axis=0, tiled=True)
    ret, tok, cot, hid, dg, du = expert(arrived, expert_gate[0], expert_up[0], expert_down[0])
    back = lax.all_to_all(ret, "sp", split_axis=0, concat_axis=0, tiled=True)
    grad_gate = contract_rows(tok, dg)[None]
    grad_up = contract_rows(tok, du)[None]
    grad_down = contract_rows(hid, cot)[None]
    gow, mid_grad, grad_b, d_conv_out = tail(
        back,
        mid_stream,
        layer_cot,
        gain,
        expert_ids,
        ids_t,
        inv,
        b_gate,
        conv_out,
        conv_gain.reshape(1, 512),
        out_weight,
    )
    parts = lax.all_to_all(gow.reshape(NDEV, 32, 512), "sp", 0, 0, tiled=True)
    grad_out_weight = jnp.sum(parts.astype(jnp.float32), axis=0)
    following = from_behind(d_conv_out[:2], "sp", -1)
    extended = jnp.concatenate([d_conv_out, following], axis=0)
    taps = conv_taps.astype(jnp.float32)
    d_mixed = taps[2] * extended[:-2] + taps[1] * extended[1:-1] + taps[0] * extended[2:]
    grad_c = (d_mixed * conv_in.astype(jnp.float32)).astype(jnp.bfloat16)
    grad_conv_in = (d_mixed * c_gate.astype(jnp.float32)).astype(jnp.bfloat16)
    return (grad_gate, grad_up, grad_down, grad_out_weight, mid_grad, grad_b, grad_c, grad_conv_in)


def solution(mesh):
    placed = (
        P("sp", "tp"),
        P("sp", "tp"),
        P("tp"),
        P("sp", None),
        P("sp"),
        P("sp"),
        P("sp", None, "tp"),
        P("sp", None, "tp"),
        P("sp", "tp", None),
        P(None, "tp"),
        P("tp"),
        P("sp", "tp"),
        P("sp", "tp"),
        P("sp", "tp"),
        P("sp", "tp"),
        P(None, "tp"),
    )
    return jax.shard_map(
        shards,
        mesh=mesh,
        in_specs=placed,
        out_specs=(
            P("sp", None, "tp"),
            P("sp", None, "tp"),
            P("sp", "tp", None),
            P("sp", "tp"),
            P("sp", "tp"),
            P("sp", "tp"),
            P("sp", "tp"),
            P("sp", "tp"),
        ),
        check_vma=False,
    )
```

profile of v0, /device:TPU:0, one launch (start us, length us, event | category | flops | bytes accessed | tf_op | source)
XLA Modules:
  0.0 216.2 jit_solution(12462386692553986352)
XLA Ops:
  0.6 0.7 reshape.32.prob
  1.3 0.7 reshape.33.share
  2.0 0.7 reshape.31.gain
  2.7 0.8 copy.24.ids
  3.5 0.0 copy-start.5
  3.5 0.7 copy-done.5
  4.2 1.1 copy-done.8
  5.3 1.1 copy-done.10
  6.4 7.0 %prep.1 = (bf16[64,80,512]{2,1,0:T(8,128)(2,1)S(1)}, f32[320,128]{1,0:T(8,128)S(1)}) custom-call(bf16[320,1024]{1,0:T(8,128)(2,1)S(1)} %copy-done.8, bf16[320,1024]{1,0:T(8,128)(2,1)S(1)} %copy-done.10, bf16[1,1024]{1,0:T(2,128)(2,1)S(1)} %reshape.31.gain, s32[320,2]{1,0:T(8,128)S(1)} %copy.24.ids, s32[2,320]{1,0:T(2,128)S(1)} %bitcast.21, ...), custom_call_target="tpu_custom_call" | custom-call | flops 6000000000 | bytes 7000000 | tf_op jit(solution)/shard_map/prep/pallas_call | solution.py:130
  13.4 0.0 copy-start.14
  13.4 75.7 %all_to_all.15.rin = bf16[64,80,512]{2,1,0:T(8,128)(2,1)} all-to-all(bf16[64,80,512]{2,1,0:T(8,128)(2,1)S(1)} %get-tuple-element.20), channel_id=1, replica_groups=mesh['sp'=64,'tp'=2] {'sp'}, dimensions={0} | all-to-all | bytes 10485760 | tf_op jit(solution)/shard_map/all_to_all | solution.py:531
  89.1 0.0 copy-done.14
  89.1 28.0 %expert.1 = (bf16[64,80,256]{2,1,0:T(8,128)(2,1)}, bf16[1280,2048]{1,0:T(8,128)(2,1)}, bf16[1280,2048]{1,0:T(8,128)(2,1)}, bf16[1280,512]{1,0:T(8,128)(2,1)}, bf...) custom-call(bf16[64,80,512]{2,1,0:T(8,128)(2,1)} %all_to_all.15.rin, bf16[2048,512]{1,0:T(8,128)(2,1)} %bitcast.26, ...), custom_call_target="tpu_custom_call" | custom-call | flops 14000000000 | bytes 30000000 | tf_op jit(solution)/shard_map/expert/pallas_call | solution.py:333
  117.1 0.0 copy-start.20
  117.1 0.0 copy-start.19
  117.1 5.8 %all-to-all-start.1 = ((bf16[64,80,256]{2,1,0:T(8,128)(2,1)}), bf16[64,80,256]{2,1,0:T(8,128)(2,1)S(1)}, u32[]{:S(2)}, u32[]{:S(2)}) async-start(bf16[64,80,256]{2,1,0:T(8,128)(2,1)} %get-tuple-element.26), calls=%async_computation.1 | async-start | bytes 5242880 | tf_op jit(solution)/shard_map/all_to_all | solution.py:533
  122.9 0.0 copy-done.20
  122.9 0.0 copy-done.19
  123.0 0.0 copy-start.6
  123.0 7.8 %convolution_bitcast_fusion.2 = f32[1,2048,512]{2,1,0:T(8,128)} fusion(bf16[1280,2048]{1,0:T(8,128)(2,1)} %get-tuple-element.21, bf16[1280,512]{1,0:T(8,128)(2,1)} %get-tuple-element.22), kind=kOutput, calls=%fused_computation.3 | convolution fusion | flops 2684354560 | bytes 10747904 | tf_op jit(solution)/shard_map/dot_general | solution.py:497
  130.8 28.8 %all-to-all-done.1.back = bf16[64,80,256]{2,1,0:T(8,128)(2,1)S(1)} async-done(((bf16[64,80,256]{2,1,0:T(8,128)(2,1)}), bf16[64,80,256]{2,1,0:T(8,128)(2,1)S(1)}, u32[]{:S(2)}, u32[]{:S(2)}) %all-to-all-start.1) | async-done | bytes 2621472 | tf_op jit(solution)/shard_map/all_to_all | solution.py:533
  159.6 0.0 copy-done.6
  159.6 1.6 copy-done.7
  161.2 1.1 copy-done.9
  162.3 1.1 copy-done.11
  163.4 1.0 copy-done.12
  164.3 1.0 copy-done.13
  165.3 0.9 copy-done.15
  166.2 8.2 %tail.1 = (bf16[2048,512]{1,0:T(8,128)(2,1)S(1)}, bf16[320,1024]{1,0:T(8,128)(2,1)S(1)}, bf16[320,512]{1,0:T(8,128)(2,1)S(1)}, f32[320,512]{1,0:T(8,128)S(1)}) custom-call(bf16[64,80,256]{2,1,0:T(8,128)(2,1)S(1)} %all-to-all-done.1.back, bf16[320,1024]{1,0:T(8,128)(2,1)S(1)} %copy-done.9, bf16[320,1024]{1,0:T(8,128)(2,1)S(1)} %copy-done.11, ...), custom_call_target="tpu_custom_call" | custom-call | flops 5000000000 | bytes 12000000 | tf_op jit(solution)/shard_map/tail/pallas_call | solution.py:463
  174.5 0.0 copy-start
  174.5 1.3 copy-done
  175.8 0.8 copy-done.1
  176.7 0.7 copy-done.3
  177.4 5.9 %all-to-all-start.2 = ((bf16[64,32,512]{2,1,0:T(8,128)(2,1)}), bf16[64,32,512]{2,1,0:T(8,128)(2,1)S(1)}, u32[]{:S(2)}, u32[]{:S(2)}) async-start(bf16[64,32,512]{2,1,0:T(8,128)(2,1)} %bitcast.20), calls=%async_computation.2 | async-start | bytes 4194304 | tf_op jit(solution)/shard_map/all_to_all | solution.py:550
  183.2 0.0 copy-start.16
  183.2 7.9 %convolution_bitcast_fusion.1 = f32[1,2048,512]{2,1,0:T(8,128)} fusion(bf16[1280,2048]{1,0:T(8,128)(2,1)} %get-tuple-element.21, bf16[1280,512]{1,0:T(8,128)(2,1)} %get-tuple-element.23), kind=kOutput, calls=%fused_computation.2 | convolution fusion | flops 2684354560 | bytes 10747904 | tf_op jit(solution)/shard_map/dot_general | solution.py:497
  191.2 0.0 copy-done.16
  191.2 7.0 %convolution_bitcast_fusion = f32[1,512,2048]{2,1,0:T(8,128)} fusion(bf16[1280,512]{1,0:T(8,128)(2,1)S(1)} %copy-done.16, bf16[1280,2048]{1,0:T(8,128)(2,1)} %get-tuple-element.25), kind=kOutput, calls=%fused_computation.1 | convolution fusion | flops 2684354560 | bytes 10747904 | tf_op jit(solution)/shard_map/dot_general | solution.py:497
  198.1 1.4 collective-permute-start
  199.6 8.0 %collective-permute-done = f32[2,512]{1,0:T(2,128)S(1)} collective-permute-done((f32[2,512]{1,0:T(2,128)S(1)}, f32[2,512]{1,0:T(2,128)S(1)}, u32[]{:S(2)}, u32[]{:S(2)}) %collective-permute-start) | collective-permute-done | bytes 4128 | tf_op jit(solution)/shard_map/ppermute | solution.py:493
  207.7 1.0 multiply_convert_fusion
  208.7 0.0 copy-done.17
  208.7 0.8 multiply_convert_fusion.1
  209.5 4.2 %all-to-all-done.2 = bf16[64,32,512]{2,1,0:T(8,128)(2,1)S(1)} async-done(((bf16[64,32,512]{2,1,0:T(8,128)(2,1)}), bf16[64,32,512]{2,1,0:T(8,128)(2,1)S(1)}, u32[]{:S(2)}, u32[]{:S(2)}) %all-to-all-start.2) | async-done | bytes 2097184 | tf_op jit(solution)/shard_map/all_to_all | solution.py:550
  213.7 1.0 convert_reduce_fusion
  214.7 0.8 copy.29
  215.5 0.0 copy-done.4
  215.5 0.7 copy.30
  (21 shorter events, 0.1 us)
Async XLA Ops:
  3.5 0.7 copy-start.5
  4.2 1.1 copy-start.8
  5.3 1.1 copy-start.10
  13.4 75.7 %copy-start.14 = (f32[320,128]{1,0:T(8,128)}, f32[320,128]{1,0:T(8,128)S(1)}, u32[]{:S(2)}) copy-start(f32[320,128]{1,0:T(8,128)S(1)} %get-tuple-element.27.inv_in) | copy-start | bytes 491524
  117.1 5.9 %copy-start.20 = (bf16[512]{0:T(512)(128)(2,1)S(1)}, bf16[512]{0:T(512)(128)(2,1)}, u32[]{:S(2)}) copy-start(bf16[512]{0:T(512)(128)(2,1)} %param.26) | copy-start | bytes 3076
  117.1 5.9 %copy-start.19 = (bf16[3,512]{1,0:T(4,128)(2,1)S(1)}, bf16[3,512]{1,0:T(4,128)(2,1)}, u32[]{:S(2)}) copy-start(bf16[3,512]{1,0:T(4,128)(2,1)} %param.31) | copy-start | bytes 9220
  117.1 42.5 %all-to-all-start.1 = ((bf16[64,80,256]{2,1,0:T(8,128)(2,1)}), bf16[64,80,256]{2,1,0:T(8,128)(2,1)S(1)}, u32[]{:S(2)}, u32[]{:S(2)}) async-start(bf16[64,80,256]{2,1,0:T(8,128)(2,1)} %get-tuple-element.26), calls=%async_computation.1 | async-start | bytes 5242880 | tf_op jit(solution)/shard_map/all_to_all | solution.py:533
  123.0 36.6 %copy-start.6 = (s32[320,2]{0,1:T(2,128)S(1)}, s32[320,2]{0,1:T(2,128)}, u32[]{:S(2)}) copy-start(s32[320,2]{0,1:T(2,128)} %param.19) | copy-start | bytes 7684
  159.6 1.6 copy-start.7
  161.2 1.1 copy-start.9
  162.3 1.1 copy-start.11
  163.4 1.0 copy-start.12
  164.3 1.0 copy-start.13
  165.3 0.9 copy-start.15
  174.5 1.3 copy-start
  175.8 0.8 copy-start.1
  176.7 0.7 copy-start.3
  177.4 36.3 %all-to-all-start.2 = ((bf16[64,32,512]{2,1,0:T(8,128)(2,1)}), bf16[64,32,512]{2,1,0:T(8,128)(2,1)S(1)}, u32[]{:S(2)}, u32[]{:S(2)}) async-start(bf16[64,32,512]{2,1,0:T(8,128)(2,1)} %bitcast.20), calls=%async_computation.2 | async-start | bytes 4194304 | tf_op jit(solution)/shard_map/all_to_all | solution.py:550
  183.2 7.9 %copy-start.16 = (bf16[1280,512]{1,0:T(8,128)(2,1)S(1)}, bf16[1280,512]{1,0:T(8,128)(2,1)}, u32[]{:S(2)}) copy-start(bf16[1280,512]{1,0:T(8,128)(2,1)} %get-tuple-element.24) | copy-start | bytes 3932164
  191.2 16.5 %copy-start.18 = (bf16[320,512]{1,0:T(8,128)(2,1)S(1)}, bf16[320,512]{1,0:T(8,128)(2,1)}, u32[]{:S(2)}) copy-start(bf16[320,512]{1,0:T(8,128)(2,1)} %param.28) | copy-start | bytes 983044
  198.1 10.5 %copy-start.17 = (bf16[320,512]{1,0:T(8,128)(2,1)S(1)}, bf16[320,512]{1,0:T(8,128)(2,1)}, u32[]{:S(2)}) copy-start(bf16[320,512]{1,0:T(8,128)(2,1)} %param.29) | copy-start | bytes 983044
  198.1 9.5 %collective-permute-start = (f32[2,512]{1,0:T(2,128)S(1)}, f32[2,512]{1,0:T(2,128)S(1)}, u32[]{:S(2)}, u32[]{:S(2)}) collective-permute-start(f32[2,512]{1,0:T(2,128)S(1)} %slice.20), channel_id=1, source_target_pairs={{2,0},{4,2},{6,4},{8,6},{10,8},{12,10},{14,12},{16,14},{18,16},{20... | collective-permute-start | bytes 12296 | tf_op jit(solution)/shard_map/ppermute | solution.py:493
  207.7 7.0 %copy-start.2 = (bf16[320,1024]{1,0:T(8,128)(2,1)S(1)}, bf16[320,1024]{1,0:T(8,128)(2,1)}, u32[]{:S(2)}) copy-start(bf16[320,1024]{1,0:T(8,128)(2,1)} %copy-done.1) | copy-start | bytes 1966084
  208.7 6.9 %copy-start.4 = (bf16[320,512]{1,0:T(8,128)(2,1)S(1)}, bf16[320,512]{1,0:T(8,128)(2,1)}, u32[]{:S(2)}) copy-start(bf16[320,512]{1,0:T(8,128)(2,1)} %copy-done.3) | copy-start | bytes 983044
where the time goes:
time: 217 us; the launch traced here: 216 us
  blocking collectives  75.7 us (35%)
  Pallas kernels  43.2 us (20%)
  waiting for transfers between devices  41.1 us (19%)
  matrix products  22.7 us (10%)
  local copies, waits for them, and re-layouts  16.9 us (8%)
  starting transfers between devices  13.1 us (6%)
  other arithmetic  2.78 us (1%)
    all_to_all x1, blocking collectives, shards(): lax.all_to_all(packed, 'sp', split_axis=0, concat_axis=0, tiled=True)  75.7 us
    all_to_all x1, waiting for transfers between devices, shards(): back = lax.all_to_all(ret, 'sp', split_axis=0, concat_axis=0, tiled=True)  28.8 us
    pallas_call x1, Pallas kernels, expert(): pl.pallas_call(expert_kernel, name='expert', out_shape=(jax.ShapeDtypeStr...  28 us
    dot_general x3, matrix products, contract_rows(): lax.dot_general(left, right, (((0,), (0,)), ((), ())), preferred_element_...  22.7 us
    unnamed x46, local copies, waits for them, and re-layouts  14.8 us
    pallas_call x1, Pallas kernels, tail(): pl.pallas_call(tail_kernel, name='tail', out_shape=(jax.ShapeDtypeStruct(...  8.23 us
    ppermute x1, waiting for transfers between devices, from_behind(): return lax.ppermute(block, axis, route)  8.04 us
    pallas_call x1, Pallas kernels, prep(): pl.pallas_call(prep_kernel, name='prep', out_shape=(jax.ShapeDtypeStruct(...  7.01 us
  transfers between devices with their start and end apart: 3, of which 3 were waited for; matrix products, arithmetic and copies ran while one was open for 11% of the time, Pallas kernels for 0%

commit v1 on v0

v1 whole, which is shorter than its diff:
```python
import functools

import jax
import jax.numpy as jnp
from jax import lax
from jax.experimental import pallas as pl
from jax.experimental.pallas import tpu as pltpu
from jax.sharding import PartitionSpec as P

D = 2048
HALF = 1024
GROUP = 64
TOK = 320
FF = 512
NDEV = 64
ROWS = 1280
JOBS = 10
RING = 3
epsilon = 1e-06

F32 = jnp.float32
BF16 = jnp.bfloat16
MESH = pl.DeviceIdType.MESH
VM = pl.BlockSpec(memory_space=pltpu.VMEM)
ANY = pl.BlockSpec(memory_space=pl.ANY)


def mm(a, b):
    return jnp.dot(a, b, preferred_element_type=F32)


def mm_nt(a, b):
    return lax.dot_general(a, b, (((1,), (1,)), ((), ())), preferred_element_type=F32)


def mm_tn(a, b):
    return lax.dot_general(a, b, (((0,), (0,)), ((), ())), preferred_element_type=F32)


def iota(shape, dim):
    return lax.broadcasted_iota(jnp.int32, shape, dim)


def ind(mask):
    return jnp.where(mask, 1.0, 0.0)


def greet(other):
    barrier = pltpu.get_barrier_semaphore()
    pl.semaphore_signal(barrier, inc=1, device_id=other, device_id_type=MESH)
    pl.semaphore_wait(barrier, 1)


def lane_slots(ids, ids_t):
    earlier = iota((TOK, TOK), 0) < iota((TOK, TOK), 1)
    out = []
    for c in range(2):
        mine = ids_t[c : c + 1, :]
        same = ind(earlier & (ids[:, 0:1] == mine)) + ind(earlier & (ids[:, 1:2] == mine))
        rank = jnp.sum(same, axis=0, keepdims=True).astype(jnp.int32)
        out.append(mine * 32 + rank)
    return out


def row_slots(ids, ids_t):
    earlier = iota((TOK, TOK), 1) < iota((TOK, TOK), 0)
    out = []
    for c in range(2):
        mine = ids[:, c : c + 1]
        same = ind(earlier & (ids_t[0:1, :] == mine)) + ind(earlier & (ids_t[1:2, :] == mine))
        rank = jnp.sum(same, axis=1, keepdims=True).astype(jnp.int32)
        out.append(mine * 32 + rank)
    return out


def row_code(r, j):
    e = ((r // 2) % 4) * 16 + ((r // 8) % 4) * 4 + r // 32
    return e * 32 + 2 * j + r % 2


def moe_kernel(
    mid,
    cot,
    gain,
    ids,
    ids_t,
    prob,
    share,
    wg,
    wu,
    wd,
    dn,
    inv_out,
    tok_out,
    cot_out,
    hid_out,
    dg_out,
    du_out,
    sq_mine,
    sq_other,
    normed,
    lanes,
    subs,
    weights,
    mix,
    unmix,
    s0,
    r1,
    r2,
    r3,
    tok_o,
    cot_o,
    tok_p,
    cot_p,
    hid,
    dg,
    du,
    mine,
    theirs,
    got,
    t0,
    t1,
    t2,
    t3,
    rows_b,
    sq_sem,
    send,
    recv,
    local,
    psend,
    precv,
    osem,
):
    sp, tp = lax.axis_index("sp"), lax.axis_index("tp")
    zz, yy, xx = sp // 16, (sp // 4) % 4, sp % 4
    other = (sp, 1 - tp)
    own_cols = pl.ds(pl.multiple_of(tp * HALF, HALF), HALF)
    oth_cols = pl.ds(pl.multiple_of((1 - tp) * HALF, HALF), HALF)

    def peer(dim, off):
        if dim == 0:
            c = (xx + off) % 4
            return c, (zz * 16 + yy * 4 + c, tp)
        if dim == 1:
            c = (yy + off) % 4
            return c, (zz * 16 + c * 4 + xx, tp)
        c = (zz + off) % 4
        return c, (c * 16 + yy * 4 + xx, tp)

    barrier = pltpu.get_barrier_semaphore()
    pl.semaphore_signal(barrier, inc=1, device_id=other, device_id_type=MESH)
    for dim in range(3):
        for off in (1, 2, 3):
            pl.semaphore_signal(barrier, inc=1, device_id=peer(dim, off)[1], device_id_type=MESH)
    pl.semaphore_wait(barrier, 10)

    m32 = mid[...].astype(F32)
    sq = jnp.sum(m32 * m32, axis=1, keepdims=True)
    sq_mine[...] = jnp.broadcast_to(sq, (TOK, 128))
    copy = pltpu.make_async_remote_copy(
        sq_mine, sq_other, sq_sem.at[0], sq_sem.at[1], device_id=other, device_id_type=MESH
    )
    copy.start()
    l0, l1 = lane_slots(ids[...], ids_t[...])
    lanes[0:1, :] = l0
    lanes[1:2, :] = l1
    b0, b1 = row_slots(ids[...], ids_t[...])
    subs[0] = jnp.broadcast_to(b0, (TOK, 128))
    subs[1] = jnp.broadcast_to(b1, (TOK, 128))
    weights[0:1, :] = prob[...] * share[...]
    weights[1:2, :] = prob[...] * (1.0 - share[...])
    i = iota((256, 256), 0)
    c = iota((256, 256), 1)
    mix[...] = ind(c == ((i // 2) % 8) * 32 + (i // 16) * 2 + i % 2).astype(BF16)
    unmix[...] = ind(c == ((i // 2) % 16) * 16 + (i // 32) * 2 + i % 2).astype(BF16)
    dn[...] = jnp.zeros((TOK, HALF), F32)
    copy.wait()
    inv = lax.rsqrt((sq + sq_other[:, 0:1]) / D + epsilon)
    inv_out[...] = jnp.broadcast_to(inv, (TOK, 128))
    normed[...] = (m32 * inv * gain[...].astype(F32)).astype(BF16)

    def part_at(buf, lead, dim, k):
        if dim == 0:
            return buf.at[lead, k]
        if dim == 1:
            return buf.at[lead, :, k]
        return buf.at[lead, :, :, k]

    def hop(stage, j):
        src, src_lead, dst, axis, depth = (
            (s0, j % RING, r1, 0, 0),
            (r1, j, r2, 1, 1),
            (r2, j, r3, 2, 2),
            (t0, j % RING, t1, 2, 0),
            (t1, j, t2, 1, 1),
            (t2, j, t3, 0, 2),
        )[stage]
        me = (xx, yy, zz)[axis]
        copies = []
        for off in (2, 1, 3):
            there, device = peer(axis, off)
            copies.append(
                pltpu.make_async_remote_copy(
                    part_at(src, src_lead, depth, there),
                    dst.at[j, me],
                    send.at[stage, j % 2, off - 1],
                    recv.at[stage, j, off - 1],
                    device_id=device,
                    device_id_type=MESH,
                )
            )
        copies.append(
            pltpu.make_async_copy(
                part_at(src, src_lead, depth, me), dst.at[j, me], local.at[stage, j % 2]
            )
        )
        return copies

    def launch(stage, j):
        for cp in hop(stage, j):
            cp.start()

    def land(stage, j):
        for cp in hop(stage, j):
            cp.wait()

    def pair(kind, j):
        src, dst = (
            (tok_o.at[j % RING], tok_p.at[j]),
            (cot_o.at[j % RING], cot_p.at[j]),
            (theirs.at[j % RING], got.at[j]),
        )[kind]
        return pltpu.make_async_remote_copy(
            src,
            dst,
            psend.at[kind, j % 2],
            precv.at[kind, j],
            device_id=other,
            device_id_type=MESH,
        )

    def keep(j):
        rows = pl.ds(pl.multiple_of(j * 128, 128), 128)
        k = j % RING
        pairs = (
            (tok_o.at[k], tok_out.at[rows, own_cols]),
            (tok_p.at[j], tok_out.at[rows, oth_cols]),
            (cot_o.at[k], cot_out.at[rows, own_cols]),
            (cot_p.at[j], cot_out.at[rows, oth_cols]),
            (hid.at[k], hid_out.at[rows]),
            (dg.at[k], dg_out.at[rows]),
            (du.at[k], du_out.at[rows]),
        )
        return [pltpu.make_async_copy(a, b, osem.at[n, j % 2]) for n, (a, b) in enumerate(pairs)]

    def select(j):
        r = iota((128, 1), 0)
        code = row_code(r, j)
        hit0 = code == lanes[0:1, :]
        hit1 = code == lanes[1:2, :]
        pick = ind(hit0 | hit1).astype(BF16)
        weight = jnp.sum(
            jnp.where(hit0, weights[0:1, :], 0.0) + jnp.where(hit1, weights[1:2, :], 0.0),
            axis=1,
            keepdims=True,
        )
        a = mm(pick, normed[...]).astype(BF16)
        b = (mm(pick, cot[...]) * weight).astype(BF16)
        for n in range(4):
            rows = slice(n * 32, n * 32 + 32)
            stack = jnp.concatenate(
                [v[rows, p * 256 : (p + 1) * 256] for v in (a, b) for p in range(4)], axis=0
            )
            s0[j % RING, n] = mm(mix[...], stack).astype(BF16).reshape(4, 4, 16, 256)
        launch(0, j)

    def unpack(j):
        k = j % RING
        for n in range(4):
            rows = slice(n * 32, n * 32 + 32)
            v = mm(unmix[...], r3[j, n].reshape(256, 256)).astype(BF16)
            for p in range(4):
                cols = slice(p * 256, (p + 1) * 256)
                tok_o[k, rows, cols] = v[p * 32 : (p + 1) * 32]
                cot_o[k, rows, cols] = v[128 + p * 32 : 128 + (p + 1) * 32]
        pair(0, j).start()
        pair(1, j).start()

    def work(j):
        k = j % RING
        pair(0, j).wait()
        pair(1, j).wait()
        xo, xp = tok_o[k], tok_p[j]
        yo, yp = cot_o[k], cot_p[j]
        pre_g = mm(xo, wg[own_cols, :]) + mm(xp, wg[oth_cols, :])
        pre_u = mm(xo, wu[own_cols, :]) + mm(xp, wu[oth_cols, :])
        d_h = mm_nt(yo, wd[:, own_cols]) + mm_nt(yp, wd[:, oth_cols])
        sigma = jax.nn.sigmoid(pre_g)
        active = pre_g * sigma
        slope = sigma * (1.0 + pre_g * (1.0 - sigma))
        hid[k] = (active * pre_u).astype(BF16)
        g = (d_h * pre_u * slope).astype(BF16)
        u = (d_h * active).astype(BF16)
        dg[k] = g
        du[k] = u
        theirs[k] = (mm_nt(g, wg[oth_cols, :]) + mm_nt(u, wu[oth_cols, :])).astype(BF16)
        pair(2, j).start()
        mine[k] = (mm_nt(g, wg[own_cols, :]) + mm_nt(u, wu[own_cols, :])).astype(BF16)
        for cp in keep(j):
            cp.start()

    def give_back(j):
        k = j % RING
        pair(2, j).wait()
        s = (mine[k].astype(F32) + got[j].astype(F32)).astype(BF16)
        for n in range(4):
            rows = slice(n * 32, n * 32 + 32)
            stack = jnp.concatenate(
                [s[rows, p * 128 : (p + 1) * 128] for p in range(8)], axis=0
            )
            t0[k, n] = mm(mix[...], stack).astype(BF16).reshape(4, 4, 16, 128)
        launch(3, j)
        for cp in keep(j):
            cp.wait()

    def collect(j):
        for n in range(4):
            rows = slice(n * 32, n * 32 + 32)
            v = mm(unmix[...], t3[j, n].reshape(256, 128)).astype(BF16)
            for p in range(8):
                rows_b[rows, p * 128 : (p + 1) * 128] = v[p * 32 : (p + 1) * 32]
        code = row_code(iota((1, 128), 1), j)
        pick = ind((code == subs[0, :, 0:1]) | (code == subs[1, :, 0:1])).astype(BF16)
        dn[...] += mm(pick, rows_b[...])

    def step(t, carry):
        def at(lag, fn):
            j = t - lag
            pl.when((j >= 0) & (j < JOBS))(lambda: fn(j))

        def relay(stage):
            def fn(j):
                land(stage, j)
                launch(stage + 1, j)

            return fn

        def arrive(j):
            land(2, j)
            unpack(j)

        def finish(j):
            land(5, j)
            collect(j)

        at(0, select)
        at(1, relay(0))
        at(2, relay(1))
        at(3, arrive)
        at(5, give_back)
        at(6, relay(3))
        at(7, relay(4))
        at(4, work)
        at(8, finish)
        return carry

    lax.fori_loop(0, JOBS + 8, step, 0)


def moe(mid, cot, gain, ids, ids_t, prob, share, wg, wu, wd):
    return pl.pallas_call(
        moe_kernel,
        name="moe",
        out_shape=(
            jax.ShapeDtypeStruct((TOK, HALF), F32),
            jax.ShapeDtypeStruct((TOK, 128), F32),
            jax.ShapeDtypeStruct((ROWS, D), BF16),
            jax.ShapeDtypeStruct((ROWS, D), BF16),
            jax.ShapeDtypeStruct((ROWS, FF), BF16),
            jax.ShapeDtypeStruct((ROWS, FF), BF16),
            jax.ShapeDtypeStruct((ROWS, FF), BF16),
        ),
        in_specs=[VM] * 10,
        out_specs=(VM, VM, ANY, ANY, ANY, ANY, ANY),
        scratch_shapes=[
            pltpu.VMEM((TOK, 128), F32),
            pltpu.VMEM((TOK, 128), F32),
            pltpu.VMEM((TOK, HALF), BF16),
            pltpu.VMEM((8, TOK), jnp.int32),
            pltpu.VMEM((2, TOK, 128), jnp.int32),
            pltpu.VMEM((8, TOK), F32),
            pltpu.VMEM((256, 256), BF16),
            pltpu.VMEM((256, 256), BF16),
            pltpu.VMEM((RING, 4, 4, 4, 16, 256), BF16),
            pltpu.VMEM((JOBS, 4, 4, 4, 16, 256), BF16),
            pltpu.VMEM((JOBS, 4, 4, 4, 16, 256), BF16),
            pltpu.VMEM((JOBS, 4, 4, 4, 16, 256), BF16),
            pltpu.VMEM((RING, 128, HALF), BF16),
            pltpu.VMEM((RING, 128, HALF), BF16),
            pltpu.VMEM((JOBS, 128, HALF), BF16),
            pltpu.VMEM((JOBS, 128, HALF), BF16),
            pltpu.VMEM((RING, 128, FF), BF16),
            pltpu.VMEM((RING, 128, FF), BF16),
            pltpu.VMEM((RING, 128, FF), BF16),
            pltpu.VMEM((RING, 128, HALF), BF16),
            pltpu.VMEM((RING, 128, HALF), BF16),
            pltpu.VMEM((JOBS, 128, HALF), BF16),
            pltpu.VMEM((RING, 4, 4, 4, 16, 128), BF16),
            pltpu.VMEM((JOBS, 4, 4, 4, 16, 128), BF16),
            pltpu.VMEM((JOBS, 4, 4, 4, 16, 128), BF16),
            pltpu.VMEM((JOBS, 4, 4, 4, 16, 128), BF16),
            pltpu.VMEM((128, HALF), BF16),
            pltpu.SemaphoreType.DMA((2,)),
            pltpu.SemaphoreType.DMA((6, 2, 3)),
            pltpu.SemaphoreType.DMA((6, JOBS, 3)),
            pltpu.SemaphoreType.DMA((6, 2)),
            pltpu.SemaphoreType.DMA((3, 2)),
            pltpu.SemaphoreType.DMA((3, JOBS)),
            pltpu.SemaphoreType.DMA((7, 2)),
        ],
        compiler_params=pltpu.CompilerParams(
            collective_id=1, has_side_effects=True, vmem_limit_bytes=62 * 2**20
        ),
        cost_estimate=pl.CostEstimate(
            flops=20 * 10**9, bytes_accessed=30 * 10**6, transcendentals=655360
        ),
    )(mid, cot, gain, ids, ids_t, prob, share, wg, wu, wd)


def tail_kernel(
    dn,
    mid,
    cot,
    gain,
    inv_in,
    bg,
    co,
    cgain,
    ow,
    gow,
    mgrad,
    gb,
    dco,
    in_mine,
    in_other,
    mg,
    send,
    recv,
):
    sp, tp = lax.axis_index("sp"), lax.axis_index("tp")
    other = (sp, 1 - tp)
    own_rows = pl.ds(pl.multiple_of(tp * HALF, HALF), HALF)
    oth_rows = pl.ds(pl.multiple_of((1 - tp) * HALF, HALF), HALF)
    greet(other)
    g_dn = dn[...] * gain[...].astype(F32)
    m32 = mid[...].astype(F32)
    inner = jnp.sum(m32 * g_dn, axis=1, keepdims=True)
    in_mine[...] = jnp.broadcast_to(inner, (TOK, 128))
    copy = pltpu.make_async_remote_copy(
        in_mine, in_other, send.at[0], recv.at[0], device_id=other, device_id_type=MESH
    )
    copy.start()
    b32 = bg[...].astype(F32)
    y32 = co[...].astype(F32)
    cg = cgain[...].astype(F32)
    gated = b32 * y32
    same = ind(iota((512, 512), 0) // GROUP == iota((512, 512), 1) // GROUP)

    def group_mean(v):
        hi = v.astype(BF16)
        rest = v - hi.astype(F32)
        md = rest.astype(BF16)
        lo = (rest - md.astype(F32)).astype(BF16)
        ones = same.astype(BF16)
        return (mm(hi, ones) + mm(md, ones) + mm(lo, ones)) / GROUP

    rms = lax.rsqrt(group_mean(gated * gated) + epsilon)
    conv_normed = (gated * rms * cg).astype(BF16)
    copy.wait()
    inv = inv_in[:, 0:1]
    mean = (inner + in_other[:, 0:1]) / D
    total = cot[...].astype(F32) + inv * g_dn - m32 * (inv * inv * inv * mean)
    mgb = total.astype(BF16)
    mgrad[...] = mgb
    mg[tp] = mgb
    swap = pltpu.make_async_remote_copy(
        mg.at[tp], mg.at[tp], send.at[1], recv.at[1], device_id=other, device_id_type=MESH
    )
    swap.start()
    gow[own_rows, :] = mm_tn(mgb, conv_normed).astype(BF16)
    d_cn = mm(mgb, ow[own_rows, :])
    swap.wait()
    mo = mg[1 - tp]
    gow[oth_rows, :] = mm_tn(mo, conv_normed).astype(BF16)
    g_dc = cg * (d_cn + mm(mo, ow[oth_rows, :]))
    gmean = group_mean(gated * g_dc)
    d_gated = rms * g_dc - gated * (rms * rms * rms * gmean)
    gb[...] = (d_gated * y32).astype(BF16)
    dco[...] = d_gated * b32


def tail(*args):
    return pl.pallas_call(
        tail_kernel,
        name="tail",
        out_shape=(
            jax.ShapeDtypeStruct((D, 512), BF16),
            jax.ShapeDtypeStruct((TOK, HALF), BF16),
            jax.ShapeDtypeStruct((TOK, 512), BF16),
            jax.ShapeDtypeStruct((TOK, 512), F32),
        ),
        in_specs=[VM] * 9,
        out_specs=(VM,) * 4,
        scratch_shapes=[
            pltpu.VMEM((TOK, 128), F32),
            pltpu.VMEM((TOK, 128), F32),
            pltpu.VMEM((2, TOK, HALF), BF16),
            pltpu.SemaphoreType.DMA((2,)),
            pltpu.SemaphoreType.DMA((2,)),
        ],
        compiler_params=pltpu.CompilerParams(
            collective_id=2, has_side_effects=True, vmem_limit_bytes=40 * 2**20
        ),
        cost_estimate=pl.CostEstimate(
            flops=5 * 10**9, bytes_accessed=12 * 10**6, transcendentals=0
        ),
    )(*args)


def from_behind(block, axis, distance):
    devices = range(lax.axis_size(axis))
    route = [(i - distance, i) for i in devices if i - distance in devices]
    return lax.ppermute(block, axis, route)


def contract_rows(left, right):
    return lax.dot_general(
        left, right, (((0,), (0,)), ((), ())), preferred_element_type=jnp.float32
    )


def shards(
    mid_stream,
    layer_cot,
    ffn_gain,
    expert_ids,
    group_prob,
    first_share,
    expert_gate,
    expert_up,
    expert_down,
    out_weight,
    conv_gain,
    b_gate,
    c_gate,
    conv_in,
    conv_out,
    conv_taps,
):
    ids_t = expert_ids.T
    gain = ffn_gain.reshape(1, HALF)
    d_normed, inv, tok, cot, hid, dg, du = moe(
        mid_stream,
        layer_cot,
        gain,
        expert_ids,
        ids_t,
        group_prob.reshape(1, TOK),
        first_share.reshape(1, TOK),
        expert_gate[0],
        expert_up[0],
        expert_down[0],
    )
    grad_gate = contract_rows(tok, dg)[None]
    grad_up = contract_rows(tok, du)[None]
    grad_down = contract_rows(hid, cot)[None]
    gow, mid_grad, grad_b, d_conv_out = tail(
        d_normed,
        mid_stream,
        layer_cot,
        gain,
        inv,
        b_gate,
        conv_out,
        conv_gain.reshape(1, 512),
        out_weight,
    )
    parts = lax.all_to_all(gow.reshape(NDEV, 32, 512), "sp", 0, 0, tiled=True)
    grad_out_weight = jnp.sum(parts.astype(jnp.float32), axis=0)
    following = from_behind(d_conv_out[:2], "sp", -1)
    extended = jnp.concatenate([d_conv_out, following], axis=0)
    taps = conv_taps.astype(jnp.float32)
    d_mixed = taps[2] * extended[:-2] + taps[1] * extended[1:-1] + taps[0] * extended[2:]
    grad_c = (d_mixed * conv_in.astype(jnp.float32)).astype(jnp.bfloat16)
    grad_conv_in = (d_mixed * c_gate.astype(jnp.float32)).astype(jnp.bfloat16)
    return (grad_gate, grad_up, grad_down, grad_out_weight, mid_grad, grad_b, grad_c, grad_conv_in)


def solution(mesh):
    placed = (
        P("sp", "tp"),
        P("sp", "tp"),
        P("tp"),
        P("sp", None),
        P("sp"),
        P("sp"),
        P("sp", None, "tp"),
        P("sp", None, "tp"),
        P("sp", "tp", None),
        P(None, "tp"),
        P("tp"),
        P("sp", "tp"),
        P("sp", "tp"),
        P("sp", "tp"),
        P("sp", "tp"),
        P(None, "tp"),
    )
    return jax.shard_map(
        shards,
        mesh=mesh,
        in_specs=placed,
        out_specs=(
            P("sp", None, "tp"),
            P("sp", None, "tp"),
            P("sp", "tp", None),
            P("sp", "tp"),
            P("sp", "tp"),
            P("sp", "tp"),
            P("sp", "tp"),
            P("sp", "tp"),
        ),
        check_vma=False,
    )
```

time: 217 us -> 196 us (0.903)
  Pallas kernels: 43.2 us -> 142 us
  blocking collectives: 75.7 us -> 0 us
  waiting for transfers between devices: 41.1 us -> 8.32 us
  local copies, waits for them, and re-layouts: 16.9 us -> 12.4 us
  starting transfers between devices: 13.1 us -> 8.78 us
  matrix products: 22.7 us -> 18.8 us
    pallas_call x2 -> x1, Pallas kernels: 35 us -> 135 us  [moe(): pl.pallas_call(moe_kernel, name='moe', out_shape=(jax.ShapeDtypeStruct((T...]
    all_to_all x1 -> x0, blocking collectives: 75.7 us -> none  [shards(): lax.all_to_all(packed, 'sp', split_axis=0, concat_axis=0, tiled=True)]
    all_to_all x1 -> x0, waiting for transfers between devices: 28.8 us -> none  [shards(): back = lax.all_to_all(ret, 'sp', split_axis=0, concat_axis=0, tiled=True)]
    unnamed x46 -> x36, local copies, waits for them, and re-layouts: 14.8 us -> 7.94 us
    all_to_all x1 -> x0, starting transfers between devices: 5.83 us -> none  [shards(): back = lax.all_to_all(ret, 'sp', split_axis=0, concat_axis=0, tiled=True)]
    ppermute x1, waiting for transfers between devices: 8.04 us -> 3.97 us  [from_behind(): return lax.ppermute(block, axis, route)]
    dot_general x3, matrix products: 22.7 us -> 18.8 us  [contract_rows(): lax.dot_general(left, right, (((0,), (0,)), ((), ())), preferred_element_...]
  transfers between devices with their start and end apart: 3 -> 2, of which waited for: 3 -> 2; matrix products, arithmetic and copies ran while one was open for 11% -> 11% of each run, Pallas kernels for 0% -> 0%
where the time goes in v1:
time: 196 us; the launch traced here: 195 us
  Pallas kernels  142 us (72%)
  matrix products  18.8 us (10%)
  local copies, waits for them, and re-layouts  12.4 us (6%)
  starting transfers between devices  8.78 us (4%)
  waiting for transfers between devices  8.32 us (4%)
  other arithmetic  4.36 us (2%)
    pallas_call x1, Pallas kernels, moe(): pl.pallas_call(moe_kernel, name='moe', out_shape=(jax.ShapeDtypeStruct((T...  135 us
    dot_general x3, matrix products, contract_rows(): lax.dot_general(left, right, (((0,), (0,)), ((), ())), preferred_element_...  18.8 us
    unnamed x36, local copies, waits for them, and re-layouts  7.94 us
    all_to_all x1, starting transfers between devices, shards(): parts = lax.all_to_all(gow.reshape(NDEV, 32, 512), 'sp', 0, 0, tiled=True)  7.31 us
    pallas_call x1, Pallas kernels, tail(): pl.pallas_call(tail_kernel, name='tail', out_shape=(jax.ShapeDtypeStruct(...  6.18 us
    all_to_all x1, waiting for transfers between devices, shards(): parts = lax.all_to_all(gow.reshape(NDEV, 32, 512), 'sp', 0, 0, tiled=True)  4.35 us
    ppermute x1, waiting for transfers between devices, from_behind(): return lax.ppermute(block, axis, route)  3.97 us
  transfers between devices with their start and end apart: 2, of which 2 were waited for; matrix products, arithmetic and copies ran while one was open for 11% of the time, Pallas kernels for 0%

profile of v1, /device:TPU:0, one launch (start us, length us, event | category | flops | bytes accessed | tf_op | source)
XLA Modules:
  0.0 195.0 jit_solution(11656267427692005184)
XLA Ops:
  0.6 1.3 reshape.31.gain
  1.9 1.5 copy.24.ids
  3.4 1.2 reshape.32.prob
  4.6 1.2 reshape.33.share
  5.9 0.7 reshape.34.cgain
  6.6 0.0 copy-start
  6.6 0.0 copy-start.2
  6.6 0.0 copy-start.3
  6.6 0.0 copy-start.4
  6.6 135.4 %moe.1 = (f32[320,1024]{1,0:T(8,128)}, f32[320,128]{1,0:T(8,128)}, bf16[1280,2048]{1,0:T(8,128)(2,1)}, bf16[1280,2048]{1,0:T(8,128)(2,1)}, bf16[1280,512]{1,0:T(...) custom-call(bf16[320,1024]{1,0:T(8,128)(2,1)} %mid.3, bf16[320,1024]{1,0:T(8,128)(2,1)} %cot.3, ...), custom_call_target="tpu_custom_call" | custom-call | flops 20000000000 | bytes 30000000 | tf_op jit(solution)/shard_map/moe/pallas_call | solution.py:371
  142.0 0.0 copy-done
  142.0 0.0 copy-done.2
  142.0 0.0 copy-done.3
  142.0 0.0 copy-done.4
  142.0 0.0 copy-start.1
  142.1 1.6 copy-done.1
  143.6 1.0 copy-done.5
  144.6 0.0 copy-start.6
  144.6 1.3 copy-done.6
  145.9 0.9 copy-done.7
  146.8 6.2 %tail.1 = (bf16[2048,512]{1,0:T(8,128)(2,1)}, bf16[320,1024]{1,0:T(8,128)(2,1)S(1)}, bf16[320,512]{1,0:T(8,128)(2,1)S(1)}, f32[320,512]{1,0:T(8,128)S(1)}) custom-call(f32[320,1024]{1,0:T(8,128)S(1)} %copy-done.6, bf16[320,1024]{1,0:T(8,128)(2,1)S(1)} %copy-done.2, bf16[320,1024]{1,0:T(8,128)(2,1)S(1)} %copy-done.3, bf16[1,1024]{1,0:T(2,128)(2,1)S(1)} %copy-done, ...), custom_call_target="tpu_custom_call" | custom-call | flops 5000000000 | bytes 12000000 | tf_op jit(solution)/shard_map/tail/pallas_call | solution.py:503
  153.0 0.0 copy-start.11
  153.0 0.0 copy-start.13
  153.1 7.3 %all-to-all-start = ((bf16[64,32,512]{2,1,0:T(8,128)(2,1)}), bf16[64,32,512]{2,1,0:T(8,128)(2,1)}, u32[]{:S(2)}, u32[]{:S(2)}) async-start(bf16[64,32,512]{2,1,0:T(8,128)(2,1)} %bitcast.7), calls=%async_computation | async-start | bytes 4194304 | tf_op jit(solution)/shard_map/all_to_all | solution.py:588
  160.4 1.5 collective-permute-start
  161.9 0.0 copy-done.11
  161.9 0.0 copy-done.13
  161.9 0.0 copy-start.12
  161.9 0.0 slice-start
  161.9 7.2 %convolution_bitcast_fusion.2 = f32[1,2048,512]{2,1,0:T(8,128)} fusion(bf16[1280,2048]{1,0:T(8,128)(2,1)} %get-tuple-element.19, bf16[1280,512]{1,0:T(8,128)(2,1)S(1)} %copy-done.13), kind=kOutput, calls=%fused_computation.3 | convolution fusion | flops 2684354560 | bytes 10747904 | tf_op jit(solution)/shard_map/dot_general | solution.py:537
  169.1 0.0 copy-done.12
  169.1 0.0 copy-start.8
  169.1 7.2 %convolution_bitcast_fusion.1 = f32[1,2048,512]{2,1,0:T(8,128)} fusion(bf16[1280,2048]{1,0:T(8,128)(2,1)} %get-tuple-element.19, bf16[1280,512]{1,0:T(8,128)(2,1)S(1)} %copy-done.12), kind=kOutput, calls=%fused_computation.2 | convolution fusion | flops 2684354560 | bytes 10747904 | tf_op jit(solution)/shard_map/dot_general | solution.py:537
  176.3 0.0 slice-done
  176.3 0.0 slice-done.1
  176.3 0.0 copy-done.8
  176.3 0.0 copy-start.10
  176.3 4.4 %convolution_bitcast_fusion = f32[1,512,2048]{2,1,0:T(8,128)} fusion(bf16[1280,512]{1,0:T(8,128)(2,1)S(1)} %copy-done.8, bf16[1280,2048]{1,0:T(8,128)(2,1)S(1)} %bitcast.21), kind=kOutput, calls=%fused_computation.1 | convolution fusion | flops 2684354560 | bytes 10747904 | tf_op jit(solution)/shard_map/dot_general | solution.py:537
  180.7 0.0 copy-start.9
  180.8 4.0 %collective-permute-done = f32[2,512]{1,0:T(2,128)S(1)} collective-permute-done((f32[2,512]{1,0:T(2,128)S(1)}, f32[2,512]{1,0:T(2,128)S(1)}, u32[]{:S(2)}, u32[]{:S(2)}) %collective-permute-start) | collective-permute-done | bytes 4128 | tf_op jit(solution)/shard_map/ppermute | solution.py:533
  184.7 0.0 copy-done.10
  184.7 1.0 multiply_convert_fusion
  185.7 0.0 copy-done.9
  185.7 0.8 multiply_convert_fusion.1
  186.6 4.4 %all-to-all-done = bf16[64,32,512]{2,1,0:T(8,128)(2,1)} async-done(((bf16[64,32,512]{2,1,0:T(8,128)(2,1)}), bf16[64,32,512]{2,1,0:T(8,128)(2,1)}, u32[]{:S(2)}, u32[]{:S(2)}) %all-to-all-start) | async-done | bytes 2097184 | tf_op jit(solution)/shard_map/all_to_all | solution.py:588
  190.9 2.5 %convert_reduce_fusion = f32[32,512]{1,0:T(8,128)} fusion(bf16[64,32,512]{2,1,0:T(8,128)(2,1)} %all-to-all-done), kind=kLoop, calls=%fused_computation | loop fusion | flops 2080768 | bytes 2162688 | tf_op jit(solution)/shard_map/reduce_sum | solution.py:589
  193.5 0.8 copy.28
  194.3 0.7 copy.29
  (8 shorter events, 0.1 us)
Async XLA Ops:
  6.6 135.4 %copy-start = (bf16[1,1024]{1,0:T(2,128)(2,1)S(1)}, bf16[1,1024]{1,0:T(2,128)(2,1)}, u32[]{:S(2)}) copy-start(bf16[1,1024]{1,0:T(2,128)(2,1)} %reshape.31.gain) | copy-start | bytes 6148
  6.6 135.4 %copy-start.2 = (bf16[320,1024]{1,0:T(8,128)(2,1)S(1)}, bf16[320,1024]{1,0:T(8,128)(2,1)}, u32[]{:S(2)}) copy-start(bf16[320,1024]{1,0:T(8,128)(2,1)} %mid.3) | copy-start | bytes 1966084
  6.6 135.4 %copy-start.3 = (bf16[320,1024]{1,0:T(8,128)(2,1)S(1)}, bf16[320,1024]{1,0:T(8,128)(2,1)}, u32[]{:S(2)}) copy-start(bf16[320,1024]{1,0:T(8,128)(2,1)} %cot.3) | copy-start | bytes 1966084
  6.6 135.5 %copy-start.4 = (bf16[320,512]{1,0:T(8,128)(2,1)S(1)}, bf16[320,512]{1,0:T(8,128)(2,1)}, u32[]{:S(2)}) copy-start(bf16[320,512]{1,0:T(8,128)(2,1)} %bg.1) | copy-start | bytes 983044
  142.0 1.6 copy-start.1
  143.6 1.0 copy-start.5
  144.6 1.3 copy-start.6
  145.9 0.9 copy-start.7
  153.0 8.8 %copy-start.11 = (bf16[3,512]{1,0:T(4,128)(2,1)S(1)}, bf16[3,512]{1,0:T(4,128)(2,1)}, u32[]{:S(2)}) copy-start(bf16[3,512]{1,0:T(4,128)(2,1)} %param.31) | copy-start | bytes 9220
  153.0 8.8 %copy-start.13 = (bf16[1280,512]{1,0:T(8,128)(2,1)S(1)}, bf16[1280,512]{1,0:T(8,128)(2,1)}, u32[]{:S(2)}) copy-start(bf16[1280,512]{1,0:T(8,128)(2,1)} %get-tuple-element.20) | copy-start | bytes 3932164
  153.1 37.9 %all-to-all-start = ((bf16[64,32,512]{2,1,0:T(8,128)(2,1)}), bf16[64,32,512]{2,1,0:T(8,128)(2,1)}, u32[]{:S(2)}, u32[]{:S(2)}) async-start(bf16[64,32,512]{2,1,0:T(8,128)(2,1)} %bitcast.7), calls=%async_computation | async-start | bytes 4194304 | tf_op jit(solution)/shard_map/all_to_all | solution.py:588
  160.4 24.3 %collective-permute-start = (f32[2,512]{1,0:T(2,128)S(1)}, f32[2,512]{1,0:T(2,128)S(1)}, u32[]{:S(2)}, u32[]{:S(2)}) collective-permute-start(f32[2,512]{1,0:T(2,128)S(1)} %slice.20), channel_id=1, source_target_pairs={{2,0},{4,2},{6,4},{8,6},{10,8},{12,10},{14,12},{16,14},{18,16},{20... | collective-permute-start | bytes 12296 | tf_op jit(solution)/shard_map/ppermute | solution.py:533
  161.9 7.2 %copy-start.12 = (bf16[1280,512]{1,0:T(8,128)(2,1)S(1)}, bf16[1280,512]{1,0:T(8,128)(2,1)}, u32[]{:S(2)}) copy-start(bf16[1280,512]{1,0:T(8,128)(2,1)} %get-tuple-element.21) | copy-start | bytes 3932164
  161.9 14.4 %slice-start = ((s8[5242880]{0:T(1024)(128)(4,1)}), s8[4194304]{0:T(1024)(128)(4,1)S(1)}, s32[]{:S(2)}) async-start(s8[5242880]{0:T(1024)(128)(4,1)} %bitcast.20), calls=%async_computation.1 | async-start | bytes 8388608
  169.1 7.2 %slice-start.1 = ((s8[5242880]{0:T(1024)(128)(4,1)}), s8[1048576]{0:T(1024)(128)(4,1)S(1)}, s32[]{:S(2)}) async-start(s8[5242880]{0:T(1024)(128)(4,1)} %bitcast.20), calls=%async_computation.2 | async-start | bytes 2097152
  169.1 7.2 %copy-start.8 = (bf16[1280,512]{1,0:T(8,128)(2,1)S(1)}, bf16[1280,512]{1,0:T(8,128)(2,1)}, u32[]{:S(2)}) copy-start(bf16[1280,512]{1,0:T(8,128)(2,1)} %get-tuple-element.22) | copy-start | bytes 3932164
  176.3 8.5 %copy-start.10 = (bf16[320,512]{1,0:T(8,128)(2,1)S(1)}, bf16[320,512]{1,0:T(8,128)(2,1)}, u32[]{:S(2)}) copy-start(bf16[320,512]{1,0:T(8,128)(2,1)} %param.28) | copy-start | bytes 983044
  180.7 5.0 %copy-start.9 = (bf16[320,512]{1,0:T(8,128)(2,1)S(1)}, bf16[320,512]{1,0:T(8,128)(2,1)}, u32[]{:S(2)}) copy-start(bf16[320,512]{1,0:T(8,128)(2,1)} %param.29) | copy-start | bytes 983044

commit v2 on v1

--- a/solution.py
+++ b/solution.py
@@ -73,8 +73,13 @@
     return out
 
 
+def stride_of(dim):
+    return (9 * dim * dim - 3 * dim + 2) // 2
+
+
 def row_code(r, j):
-    e = ((r // 2) % 4) * 16 + ((r // 8) % 4) * 4 + r // 32
+    a, b, c = (stride_of((j + phase) % 3) for phase in range(3))
+    e = ((r // 2) % 4) * c + ((r // 8) % 4) * b + (r // 32) * a
     return e * 32 + 2 * j + r % 2
 
 
@@ -82,13 +87,12 @@
     mid,
     cot,
     gain,
-    ids,
     ids_t,
     prob,
     share,
-    wg,
-    wu,
-    wd,
+    wg_in,
+    wu_in,
+    wd_in,
     dn,
     inv_out,
     tok_out,
@@ -123,6 +127,9 @@
     t2,
     t3,
     rows_b,
+    wg,
+    wu,
+    wd,
     sq_sem,
     send,
     recv,
@@ -130,80 +137,86 @@
     psend,
     precv,
     osem,
+    wsem,
 ):
     sp, tp = lax.axis_index("sp"), lax.axis_index("tp")
-    zz, yy, xx = sp // 16, (sp // 4) % 4, sp % 4
     other = (sp, 1 - tp)
     own_cols = pl.ds(pl.multiple_of(tp * HALF, HALF), HALF)
     oth_cols = pl.ds(pl.multiple_of((1 - tp) * HALF, HALF), HALF)
 
+    def place(dim):
+        return (sp // stride_of(dim)) % 4
+
     def peer(dim, off):
-        if dim == 0:
-            c = (xx + off) % 4
-            return c, (zz * 16 + yy * 4 + c, tp)
-        if dim == 1:
-            c = (yy + off) % 4
-            return c, (zz * 16 + c * 4 + xx, tp)
-        c = (zz + off) % 4
-        return c, (c * 16 + yy * 4 + xx, tp)
+        c = (place(dim) + off) % 4
+        return c, (sp + (c - place(dim)) * stride_of(dim), tp)
 
     barrier = pltpu.get_barrier_semaphore()
     pl.semaphore_signal(barrier, inc=1, device_id=other, device_id_type=MESH)
     for dim in range(3):
         for off in (1, 2, 3):
             pl.semaphore_signal(barrier, inc=1, device_id=peer(dim, off)[1], device_id_type=MESH)
-    pl.semaphore_wait(barrier, 10)
-
+    loads = [
+        pltpu.make_async_copy(a, b, wsem.at[n])
+        for n, (a, b) in enumerate(((wg_in, wg), (wu_in, wu), (wd_in, wd)))
+    ]
+    for cp in loads:
+        cp.start()
     m32 = mid[...].astype(F32)
     sq = jnp.sum(m32 * m32, axis=1, keepdims=True)
     sq_mine[...] = jnp.broadcast_to(sq, (TOK, 128))
-    copy = pltpu.make_async_remote_copy(
-        sq_mine, sq_other, sq_sem.at[0], sq_sem.at[1], device_id=other, device_id_type=MESH
-    )
-    copy.start()
-    l0, l1 = lane_slots(ids[...], ids_t[...])
+    eye = ind(iota((TOK, TOK), 0) == iota((TOK, TOK), 1)).astype(BF16)
+    ids = mm_nt(eye, ids_t[...].astype(F32).astype(BF16)).astype(jnp.int32)
+    l0, l1 = lane_slots(ids, ids_t[...])
     lanes[0:1, :] = l0
     lanes[1:2, :] = l1
-    b0, b1 = row_slots(ids[...], ids_t[...])
-    subs[0] = jnp.broadcast_to(b0, (TOK, 128))
-    subs[1] = jnp.broadcast_to(b1, (TOK, 128))
     weights[0:1, :] = prob[...] * share[...]
     weights[1:2, :] = prob[...] * (1.0 - share[...])
     i = iota((256, 256), 0)
     c = iota((256, 256), 1)
     mix[...] = ind(c == ((i // 2) % 8) * 32 + (i // 16) * 2 + i % 2).astype(BF16)
+    dn[...] = jnp.zeros((TOK, HALF), F32)
+    pl.semaphore_wait(barrier, 10)
+    copy = pltpu.make_async_remote_copy(
+        sq_mine, sq_other, sq_sem.at[0], sq_sem.at[1], device_id=other, device_id_type=MESH
+    )
+    copy.start()
+    b0, b1 = row_slots(ids, ids_t[...])
+    subs[0] = jnp.broadcast_to(b0, (TOK, 128))
+    subs[1] = jnp.broadcast_to(b1, (TOK, 128))
     unmix[...] = ind(c == ((i // 2) % 16) * 16 + (i // 32) * 2 + i % 2).astype(BF16)
-    dn[...] = jnp.zeros((TOK, HALF), F32)
     copy.wait()
     inv = lax.rsqrt((sq + sq_other[:, 0:1]) / D + epsilon)
     inv_out[...] = jnp.broadcast_to(inv, (TOK, 128))
     normed[...] = (m32 * inv * gain[...].astype(F32)).astype(BF16)
 
-    def part_at(buf, lead, dim, k):
-        if dim == 0:
+    def part_at(buf, lead, depth, k):
+        if depth == 0:
             return buf.at[lead, k]
-        if dim == 1:
+        if depth == 1:
             return buf.at[lead, :, k]
         return buf.at[lead, :, :, k]
 
     def hop(stage, j):
-        src, src_lead, dst, axis, depth = (
-            (s0, j % RING, r1, 0, 0),
-            (r1, j, r2, 1, 1),
-            (r2, j, r3, 2, 2),
-            (t0, j % RING, t1, 2, 0),
-            (t1, j, t2, 1, 1),
-            (t2, j, t3, 0, 2),
+        src, lead, dst = (
+            (s0, j % 6, r1),
+            (r1, j, r2),
+            (r2, j, r3),
+            (t0, (j + 2) % RING, t1),
+            (t1, j, t2),
+            (t2, j, t3),
         )[stage]
-        me = (xx, yy, zz)[axis]
+        dim = (j + (0, 1, 2, 2, 1, 0)[stage]) % 3
+        depth = stage % 3
+        me = place(dim)
         copies = []
         for off in (2, 1, 3):
-            there, device = peer(axis, off)
+            there, device = peer(dim, off)
             copies.append(
                 pltpu.make_async_remote_copy(
-                    part_at(src, src_lead, depth, there),
+                    part_at(src, lead, depth, there),
                     dst.at[j, me],
-                    send.at[stage, j % 2, off - 1],
+                    send.at[stage, j % 6, off - 1],
                     recv.at[stage, j, off - 1],
                     device_id=device,
                     device_id_type=MESH,
@@ -211,7 +224,7 @@
             )
         copies.append(
             pltpu.make_async_copy(
-                part_at(src, src_lead, depth, me), dst.at[j, me], local.at[stage, j % 2]
+                part_at(src, lead, depth, me), dst.at[j, me], local.at[stage, j % 6]
             )
         )
         return copies
@@ -226,14 +239,14 @@
 
     def pair(kind, j):
         src, dst = (
-            (tok_o.at[j % RING], tok_p.at[j]),
-            (cot_o.at[j % RING], cot_p.at[j]),
-            (theirs.at[j % RING], got.at[j]),
+            (tok_o.at[(j + 2) % RING], tok_p.at[j]),
+            (cot_o.at[(j + 2) % RING], cot_p.at[j]),
+            (theirs.at[(j + 2) % RING], got.at[j]),
         )[kind]
         return pltpu.make_async_remote_copy(
             src,
             dst,
-            psend.at[kind, j % 2],
+            psend.at[kind, j % RING],
             precv.at[kind, j],
             device_id=other,
             device_id_type=MESH,
@@ -241,7 +254,7 @@
 
     def keep(j):
         rows = pl.ds(pl.multiple_of(j * 128, 128), 128)
-        k = j % RING
+        k = (j + 2) % RING
         pairs = (
             (tok_o.at[k], tok_out.at[rows, own_cols]),
             (tok_p.at[j], tok_out.at[rows, oth_cols]),
@@ -251,7 +264,7 @@
             (dg.at[k], dg_out.at[rows]),
             (du.at[k], du_out.at[rows]),
         )
-        return [pltpu.make_async_copy(a, b, osem.at[n, j % 2]) for n, (a, b) in enumerate(pairs)]
+        return [pltpu.make_async_copy(a, b, osem.at[n, j % RING]) for n, (a, b) in enumerate(pairs)]
 
     def select(j):
         r = iota((128, 1), 0)
@@ -271,11 +284,16 @@
             stack = jnp.concatenate(
                 [v[rows, p * 256 : (p + 1) * 256] for v in (a, b) for p in range(4)], axis=0
             )
-            s0[j % RING, n] = mm(mix[...], stack).astype(BF16).reshape(4, 4, 16, 256)
+            s0[j % 6, n] = mm(mix[...], stack).astype(BF16).reshape(4, 4, 16, 256)
         launch(0, j)
 
+    def settle(j):
+        for cp in keep(j):
+            cp.wait()
+
     def unpack(j):
-        k = j % RING
+        k = (j + 2) % RING
+        pl.when(j >= RING)(lambda: settle(j - RING))
         for n in range(4):
             rows = slice(n * 32, n * 32 + 32)
             v = mm(unmix[...], r3[j, n].reshape(256, 256)).astype(BF16)
@@ -286,31 +304,41 @@
         pair(0, j).start()
         pair(1, j).start()
 
-    def work(j):
-        k = j % RING
-        pair(0, j).wait()
-        pair(1, j).wait()
-        xo, xp = tok_o[k], tok_p[j]
-        yo, yp = cot_o[k], cot_p[j]
-        pre_g = mm(xo, wg[own_cols, :]) + mm(xp, wg[oth_cols, :])
-        pre_u = mm(xo, wu[own_cols, :]) + mm(xp, wu[oth_cols, :])
-        d_h = mm_nt(yo, wd[:, own_cols]) + mm_nt(yp, wd[:, oth_cols])
+    def work(j0, n):
+        m = n * 128
+        ring = pl.ds(2 if n == 1 else 0, n)
+        jobs = pl.ds(j0, n)
+        xo, yo = tok_o[ring].reshape(m, HALF), cot_o[ring].reshape(m, HALF)
+        pre_g = mm(xo, wg[own_cols, :])
+        pre_u = mm(xo, wu[own_cols, :])
+        d_h = mm_nt(yo, wd[:, own_cols])
+        for d in range(n):
+            pair(0, j0 + d).wait()
+            pair(1, j0 + d).wait()
+        xp, yp = tok_p[jobs].reshape(m, HALF), cot_p[jobs].reshape(m, HALF)
+        pre_g += mm(xp, wg[oth_cols, :])
+        pre_u += mm(xp, wu[oth_cols, :])
+        d_h += mm_nt(yp, wd[:, oth_cols])
         sigma = jax.nn.sigmoid(pre_g)
         active = pre_g * sigma
         slope = sigma * (1.0 + pre_g * (1.0 - sigma))
-        hid[k] = (active * pre_u).astype(BF16)
+        hid[ring] = (active * pre_u).astype(BF16).reshape(n, 128, FF)
         g = (d_h * pre_u * slope).astype(BF16)
         u = (d_h * active).astype(BF16)
-        dg[k] = g
-        du[k] = u
-        theirs[k] = (mm_nt(g, wg[oth_cols, :]) + mm_nt(u, wu[oth_cols, :])).astype(BF16)
-        pair(2, j).start()
-        mine[k] = (mm_nt(g, wg[own_cols, :]) + mm_nt(u, wu[own_cols, :])).astype(BF16)
-        for cp in keep(j):
-            cp.start()
+        dg[ring] = g.reshape(n, 128, FF)
+        du[ring] = u.reshape(n, 128, FF)
+        back = mm_nt(g, wg[oth_cols, :]) + mm_nt(u, wu[oth_cols, :])
+        theirs[ring] = back.astype(BF16).reshape(n, 128, HALF)
+        for d in range(n):
+            pair(2, j0 + d).start()
+        back = mm_nt(g, wg[own_cols, :]) + mm_nt(u, wu[own_cols, :])
+        mine[ring] = back.astype(BF16).reshape(n, 128, HALF)
+        for d in range(n):
+            for cp in keep(j0 + d):
+                cp.start()
 
     def give_back(j):
-        k = j % RING
+        k = (j + 2) % RING
         pair(2, j).wait()
         s = (mine[k].astype(F32) + got[j].astype(F32)).astype(BF16)
         for n in range(4):
@@ -320,8 +348,6 @@
             )
             t0[k, n] = mm(mix[...], stack).astype(BF16).reshape(4, 4, 16, 128)
         launch(3, j)
-        for cp in keep(j):
-            cp.wait()
 
     def collect(j):
         for n in range(4):
@@ -333,41 +359,52 @@
         pick = ind((code == subs[0, :, 0:1]) | (code == subs[1, :, 0:1])).astype(BF16)
         dn[...] += mm(pick, rows_b[...])
 
+    def relay(stage):
+        def fn(j):
+            land(stage, j)
+            launch(stage + 1, j)
+
+        return fn
+
+    def arrive(j):
+        land(2, j)
+        unpack(j)
+
+    def finish(j):
+        land(5, j)
+        collect(j)
+
+    def trio(group, fn):
+        def one(c, carry):
+            j = group * 3 - 2 + c
+            pl.when((j >= 0) & (j < JOBS))(lambda: fn(j))
+            return carry
+
+        lax.fori_loop(0, 3, one, 0)
+
     def step(t, carry):
-        def at(lag, fn):
-            j = t - lag
-            pl.when((j >= 0) & (j < JOBS))(lambda: fn(j))
-
-        def relay(stage):
-            def fn(j):
-                land(stage, j)
-                launch(stage + 1, j)
-
-            return fn
-
-        def arrive(j):
-            land(2, j)
-            unpack(j)
-
-        def finish(j):
-            land(5, j)
-            collect(j)
-
-        at(0, select)
-        at(1, relay(0))
-        at(2, relay(1))
-        at(3, arrive)
-        at(5, give_back)
-        at(6, relay(3))
-        at(7, relay(4))
-        at(4, work)
-        at(8, finish)
+        trio(t - 5, relay(4))
+        trio(t - 4, relay(3))
+        trio(t - 2, relay(1))
+        trio(t - 1, relay(0))
+        trio(t + 1, select)
+        trio(t - 3, arrive)
+        pl.when(t == 3)(lambda: work(0, 1))
+        pl.when((t > 3) & (t < 7))(lambda: work(3 * t - 11, 3))
+        trio(t - 6, finish)
+        trio(t - 3, give_back)
         return carry
 
-    lax.fori_loop(0, JOBS + 8, step, 0)
-
-
-def moe(mid, cot, gain, ids, ids_t, prob, share, wg, wu, wd):
+    select(0)
+    trio(1, select)
+    for cp in loads:
+        cp.wait()
+    lax.fori_loop(1, 10, step, 0)
+    for j in range(JOBS - RING, JOBS):
+        settle(j)
+
+
+def moe(mid, cot, gain, ids_t, prob, share, wg, wu, wd):
     return pl.pallas_call(
         moe_kernel,
         name="moe",
@@ -380,7 +417,7 @@
             jax.ShapeDtypeStruct((ROWS, FF), BF16),
             jax.ShapeDtypeStruct((ROWS, FF), BF16),
         ),
-        in_specs=[VM] * 10,
+        in_specs=[VM] * 6 + [ANY] * 3,
         out_specs=(VM, VM, ANY, ANY, ANY, ANY, ANY),
         scratch_shapes=[
             pltpu.VMEM((TOK, 128), F32),
@@ -391,7 +428,7 @@
             pltpu.VMEM((8, TOK), F32),
             pltpu.VMEM((256, 256), BF16),
             pltpu.VMEM((256, 256), BF16),
-            pltpu.VMEM((RING, 4, 4, 4, 16, 256), BF16),
+            pltpu.VMEM((6, 4, 4, 4, 16, 256), BF16),
             pltpu.VMEM((JOBS, 4, 4, 4, 16, 256), BF16),
             pltpu.VMEM((JOBS, 4, 4, 4, 16, 256), BF16),
             pltpu.VMEM((JOBS, 4, 4, 4, 16, 256), BF16),
@@ -410,13 +447,17 @@
             pltpu.VMEM((JOBS, 4, 4, 4, 16, 128), BF16),
             pltpu.VMEM((JOBS, 4, 4, 4, 16, 128), BF16),
             pltpu.VMEM((128, HALF), BF16),
+            pltpu.VMEM((D, FF), BF16),
+            pltpu.VMEM((D, FF), BF16),
+            pltpu.VMEM((FF, D), BF16),
             pltpu.SemaphoreType.DMA((2,)),
-            pltpu.SemaphoreType.DMA((6, 2, 3)),
+            pltpu.SemaphoreType.DMA((6, 6, 3)),
             pltpu.SemaphoreType.DMA((6, JOBS, 3)),
-            pltpu.SemaphoreType.DMA((6, 2)),
-            pltpu.SemaphoreType.DMA((3, 2)),
+            pltpu.SemaphoreType.DMA((6, 6)),
+            pltpu.SemaphoreType.DMA((3, RING)),
             pltpu.SemaphoreType.DMA((3, JOBS)),
-            pltpu.SemaphoreType.DMA((7, 2)),
+            pltpu.SemaphoreType.DMA((7, RING)),
+            pltpu.SemaphoreType.DMA((3,)),
         ],
         compiler_params=pltpu.CompilerParams(
             collective_id=1, has_side_effects=True, vmem_limit_bytes=62 * 2**20
@@ -424,7 +465,7 @@
         cost_estimate=pl.CostEstimate(
             flops=20 * 10**9, bytes_accessed=30 * 10**6, transcendentals=655360
         ),
-    )(mid, cot, gain, ids, ids_t, prob, share, wg, wu, wd)
+    )(mid, cot, gain, ids_t, prob, share, wg, wu, wd)
 
 
 def tail_kernel(
@@ -557,14 +598,12 @@
     conv_out,
     conv_taps,
 ):
-    ids_t = expert_ids.T
     gain = ffn_gain.reshape(1, HALF)
     d_normed, inv, tok, cot, hid, dg, du = moe(
         mid_stream,
         layer_cot,
         gain,
-        expert_ids,
-        ids_t,
+        expert_ids.T,
         group_prob.reshape(1, TOK),
         first_share.reshape(1, TOK),
         expert_gate[0],

time: 196 us -> 186 us (0.949)
  Pallas kernels: 142 us -> 134 us
    pallas_call x1, Pallas kernels: 135 us -> 128 us  [moe(): pl.pallas_call(moe_kernel, name='moe', out_shape=(jax.ShapeDtypeStruct((T...]
    unnamed x36 -> x35, local copies, waits for them, and re-layouts: 7.94 us -> 6.45 us
where the time goes in v2:
time: 186 us; the launch traced here: 185 us
  Pallas kernels  134 us (72%)
  matrix products  18.8 us (10%)
  local copies, waits for them, and re-layouts  10.9 us (6%)
  waiting for transfers between devices  8.5 us (5%)
  starting transfers between devices  7.79 us (4%)
  other arithmetic  4.36 us (2%)
    pallas_call x1, Pallas kernels, moe(): pl.pallas_call(moe_kernel, name='moe', out_shape=(jax.ShapeDtypeStruct((T...  128 us
    dot_general x3, matrix products, contract_rows(): lax.dot_general(left, right, (((0,), (0,)), ((), ())), preferred_element_...  18.8 us
    all_to_all x1, starting transfers between devices, shards(): parts = lax.all_to_all(gow.reshape(NDEV, 32, 512), 'sp', 0, 0, tiled=True)  6.5 us
    unnamed x35, local copies, waits for them, and re-layouts  6.45 us
    pallas_call x1, Pallas kernels, tail(): pl.pallas_call(tail_kernel, name='tail', out_shape=(jax.ShapeDtypeStruct(...  6.19 us
    all_to_all x1, waiting for transfers between devices, shards(): parts = lax.all_to_all(gow.reshape(NDEV, 32, 512), 'sp', 0, 0, tiled=True)  4.35 us
    ppermute x1, waiting for transfers between devices, from_behind(): return lax.ppermute(block, axis, route)  4.15 us
  transfers between devices with their start and end apart: 2, of which 2 were waited for; matrix products, arithmetic and copies ran while one was open for 11% of the time, Pallas kernels for 0%

profile of v2, /device:TPU:0, one launch (start us, length us, event | category | flops | bytes accessed | tf_op | source)
XLA Modules:
  0.0 185.2 jit_solution(7323777701680157916)
XLA Ops:
  0.6 1.3 reshape.31.gain
  1.9 1.2 reshape.32.prob
  3.2 1.2 reshape.33.share
  4.4 0.7 reshape.34.cgain
  5.1 0.0 copy-start
  5.1 0.0 copy-start.2
  5.1 0.0 copy-start.3
  5.1 0.0 copy-start.4
  5.1 127.9 %moe.1 = (f32[320,1024]{1,0:T(8,128)}, f32[320,128]{1,0:T(8,128)}, bf16[1280,2048]{1,0:T(8,128)(2,1)}, bf16[1280,2048]{1,0:T(8,128)(2,1)}, bf16[1280,512]{1,0:T(...) custom-call(bf16[320,1024]{1,0:T(8,128)(2,1)} %mid.3, bf16[320,1024]{1,0:T(8,128)(2,1)} %cot.3, ...), custom_call_target="tpu_custom_call" | custom-call | flops 20000000000 | bytes 30000000 | tf_op jit(solution)/shard_map/moe/pallas_call | solution.py:408
  133.0 0.0 copy-done
  133.0 0.0 copy-done.2
  133.1 0.0 copy-done.3
  133.1 0.0 copy-done.4
  133.1 0.0 copy-start.1
  133.1 1.6 copy-done.1
  134.7 0.0 copy-start.5
  134.7 1.0 copy-done.5
  135.6 0.0 copy-start.6
  135.6 1.3 copy-done.6
  137.0 0.0 copy-start.7
  137.0 0.9 copy-done.7
  137.9 6.2 %tail.1 = (bf16[2048,512]{1,0:T(8,128)(2,1)}, bf16[320,1024]{1,0:T(8,128)(2,1)S(1)}, bf16[320,512]{1,0:T(8,128)(2,1)S(1)}, f32[320,512]{1,0:T(8,128)S(1)}) custom-call(f32[320,1024]{1,0:T(8,128)S(1)} %copy-done.6, bf16[320,1024]{1,0:T(8,128)(2,1)S(1)} %copy-done.2, bf16[320,1024]{1,0:T(8,128)(2,1)S(1)} %copy-done.3, bf16[1,1024]{1,0:T(2,128)(2,1)S(1)} %copy-done, ...), custom_call_target="tpu_custom_call" | custom-call | flops 5000000000 | bytes 12000000 | tf_op jit(solution)/shard_map/tail/pallas_call | solution.py:544
  144.1 0.0 copy-start.11
  144.1 0.0 copy-start.13
  144.1 6.5 %all-to-all-start = ((bf16[64,32,512]{2,1,0:T(8,128)(2,1)}), bf16[64,32,512]{2,1,0:T(8,128)(2,1)}, u32[]{:S(2)}, u32[]{:S(2)}) async-start(bf16[64,32,512]{2,1,0:T(8,128)(2,1)} %bitcast.7), calls=%async_computation | async-start | bytes 4194304 | tf_op jit(solution)/shard_map/all_to_all | solution.py:627
  150.6 1.3 collective-permute-start
  151.9 0.0 copy-done.11
  151.9 0.0 copy-done.13
  152.0 0.0 copy-start.12
  152.0 0.0 slice-start
  152.0 7.2 %convolution_bitcast_fusion.2 = f32[1,2048,512]{2,1,0:T(8,128)} fusion(bf16[1280,2048]{1,0:T(8,128)(2,1)} %get-tuple-element.19, bf16[1280,512]{1,0:T(8,128)(2,1)S(1)} %copy-done.13), kind=kOutput, calls=%fused_computation.3 | convolution fusion | flops 2684354560 | bytes 10747904 | tf_op jit(solution)/shard_map/dot_general | solution.py:578
  159.1 0.0 copy-done.12
  159.1 0.0 slice-start.1
  159.2 7.2 %convolution_bitcast_fusion.1 = f32[1,2048,512]{2,1,0:T(8,128)} fusion(bf16[1280,2048]{1,0:T(8,128)(2,1)} %get-tuple-element.19, bf16[1280,512]{1,0:T(8,128)(2,1)S(1)} %copy-done.12), kind=kOutput, calls=%fused_computation.2 | convolution fusion | flops 2684354560 | bytes 10747904 | tf_op jit(solution)/shard_map/dot_general | solution.py:578
  166.3 0.0 slice-done
  166.3 0.0 slice-done.1
  166.3 0.0 copy-done.8
  166.3 0.0 copy-start.10
  166.3 4.4 %convolution_bitcast_fusion = f32[1,512,2048]{2,1,0:T(8,128)} fusion(bf16[1280,512]{1,0:T(8,128)(2,1)S(1)} %copy-done.8, bf16[1280,2048]{1,0:T(8,128)(2,1)S(1)} %bitcast.21), kind=kOutput, calls=%fused_computation.1 | convolution fusion | flops 2684354560 | bytes 10747904 | tf_op jit(solution)/shard_map/dot_general | solution.py:578
  170.8 4.1 %collective-permute-done = f32[2,512]{1,0:T(2,128)S(1)} collective-permute-done((f32[2,512]{1,0:T(2,128)S(1)}, f32[2,512]{1,0:T(2,128)S(1)}, u32[]{:S(2)}, u32[]{:S(2)}) %collective-permute-start) | collective-permute-done | bytes 4128 | tf_op jit(solution)/shard_map/ppermute | solution.py:574
  175.0 0.0 copy-done.10
  175.0 1.0 multiply_convert_fusion
  176.0 0.0 copy-done.9
  176.0 0.8 multiply_convert_fusion.1
  176.8 4.4 %all-to-all-done = bf16[64,32,512]{2,1,0:T(8,128)(2,1)} async-done(((bf16[64,32,512]{2,1,0:T(8,128)(2,1)}), bf16[64,32,512]{2,1,0:T(8,128)(2,1)}, u32[]{:S(2)}, u32[]{:S(2)}) %all-to-all-start) | async-done | bytes 2097184 | tf_op jit(solution)/shard_map/all_to_all | solution.py:627
  181.1 2.5 %convert_reduce_fusion = f32[32,512]{1,0:T(8,128)} fusion(bf16[64,32,512]{2,1,0:T(8,128)(2,1)} %all-to-all-done), kind=kLoop, calls=%fused_computation | loop fusion | flops 2080768 | bytes 2162688 | tf_op jit(solution)/shard_map/reduce_sum | solution.py:628
  183.7 0.8 copy.27
  184.5 0.7 copy.28
  (7 shorter events, 0.1 us)
Async XLA Ops:
  5.1 128.0 %copy-start = (bf16[1,1024]{1,0:T(2,128)(2,1)S(1)}, bf16[1,1024]{1,0:T(2,128)(2,1)}, u32[]{:S(2)}) copy-start(bf16[1,1024]{1,0:T(2,128)(2,1)} %reshape.31.gain) | copy-start | bytes 6148
  5.1 128.0 %copy-start.2 = (bf16[320,1024]{1,0:T(8,128)(2,1)S(1)}, bf16[320,1024]{1,0:T(8,128)(2,1)}, u32[]{:S(2)}) copy-start(bf16[320,1024]{1,0:T(8,128)(2,1)} %mid.3) | copy-start | bytes 1966084
  5.1 128.0 %copy-start.3 = (bf16[320,1024]{1,0:T(8,128)(2,1)S(1)}, bf16[320,1024]{1,0:T(8,128)(2,1)}, u32[]{:S(2)}) copy-start(bf16[320,1024]{1,0:T(8,128)(2,1)} %cot.3) | copy-start | bytes 1966084
  5.1 128.0 %copy-start.4 = (bf16[320,512]{1,0:T(8,128)(2,1)S(1)}, bf16[320,512]{1,0:T(8,128)(2,1)}, u32[]{:S(2)}) copy-start(bf16[320,512]{1,0:T(8,128)(2,1)} %bg.1) | copy-start | bytes 983044
  133.1 1.6 copy-start.1
  134.7 1.0 copy-start.5
  135.6 1.3 copy-start.6
  137.0 0.9 copy-start.7
  144.1 7.8 %copy-start.11 = (bf16[3,512]{1,0:T(4,128)(2,1)S(1)}, bf16[3,512]{1,0:T(4,128)(2,1)}, u32[]{:S(2)}) copy-start(bf16[3,512]{1,0:T(4,128)(2,1)} %param.31) | copy-start | bytes 9220
  144.1 7.9 %copy-start.13 = (bf16[1280,512]{1,0:T(8,128)(2,1)S(1)}, bf16[1280,512]{1,0:T(8,128)(2,1)}, u32[]{:S(2)}) copy-start(bf16[1280,512]{1,0:T(8,128)(2,1)} %get-tuple-element.20) | copy-start | bytes 3932164
  144.1 37.0 %all-to-all-start = ((bf16[64,32,512]{2,1,0:T(8,128)(2,1)}), bf16[64,32,512]{2,1,0:T(8,128)(2,1)}, u32[]{:S(2)}, u32[]{:S(2)}) async-start(bf16[64,32,512]{2,1,0:T(8,128)(2,1)} %bitcast.7), calls=%async_computation | async-start | bytes 4194304 | tf_op jit(solution)/shard_map/all_to_all | solution.py:627
  150.6 24.3 %collective-permute-start = (f32[2,512]{1,0:T(2,128)S(1)}, f32[2,512]{1,0:T(2,128)S(1)}, u32[]{:S(2)}, u32[]{:S(2)}) collective-permute-start(f32[2,512]{1,0:T(2,128)S(1)} %slice.20), channel_id=1, source_target_pairs={{2,0},{4,2},{6,4},{8,6},{10,8},{12,10},{14,12},{16,14},{18,16},{20... | collective-permute-start | bytes 12296 | tf_op jit(solution)/shard_map/ppermute | solution.py:574
  152.0 7.2 %copy-start.12 = (bf16[1280,512]{1,0:T(8,128)(2,1)S(1)}, bf16[1280,512]{1,0:T(8,128)(2,1)}, u32[]{:S(2)}) copy-start(bf16[1280,512]{1,0:T(8,128)(2,1)} %get-tuple-element.21) | copy-start | bytes 3932164
  152.0 14.4 %slice-start = ((s8[5242880]{0:T(1024)(128)(4,1)}), s8[4194304]{0:T(1024)(128)(4,1)S(1)}, s32[]{:S(2)}) async-start(s8[5242880]{0:T(1024)(128)(4,1)} %bitcast.20), calls=%async_computation.1 | async-start | bytes 8388608
  159.1 7.2 %slice-start.1 = ((s8[5242880]{0:T(1024)(128)(4,1)}), s8[1048576]{0:T(1024)(128)(4,1)S(1)}, s32[]{:S(2)}) async-start(s8[5242880]{0:T(1024)(128)(4,1)} %bitcast.20), calls=%async_computation.2 | async-start | bytes 2097152
  159.1 7.2 %copy-start.8 = (bf16[1280,512]{1,0:T(8,128)(2,1)S(1)}, bf16[1280,512]{1,0:T(8,128)(2,1)}, u32[]{:S(2)}) copy-start(bf16[1280,512]{1,0:T(8,128)(2,1)} %get-tuple-element.22) | copy-start | bytes 3932164
  166.3 8.6 %copy-start.10 = (bf16[320,512]{1,0:T(8,128)(2,1)S(1)}, bf16[320,512]{1,0:T(8,128)(2,1)}, u32[]{:S(2)}) copy-start(bf16[320,512]{1,0:T(8,128)(2,1)} %param.28) | copy-start | bytes 983044
  170.8 5.2 %copy-start.9 = (bf16[320,512]{1,0:T(8,128)(2,1)S(1)}, bf16[320,512]{1,0:T(8,128)(2,1)}, u32[]{:S(2)}) copy-start(bf16[320,512]{1,0:T(8,128)(2,1)} %param.29) | copy-start | bytes 983044

commit v3 on v2

--- a/solution.py
+++ b/solution.py
@@ -170,8 +170,10 @@
     l0, l1 = lane_slots(ids, ids_t[...])
     lanes[0:1, :] = l0
     lanes[1:2, :] = l1
-    weights[0:1, :] = prob[...] * share[...]
-    weights[1:2, :] = prob[...] * (1.0 - share[...])
+    p1 = prob[...].reshape(1, TOK)
+    f1 = share[...].reshape(1, TOK)
+    weights[0:1, :] = p1 * f1
+    weights[1:2, :] = p1 * (1.0 - f1)
     i = iota((256, 256), 0)
     c = iota((256, 256), 1)
     mix[...] = ind(c == ((i // 2) % 8) * 32 + (i // 16) * 2 + i % 2).astype(BF16)
@@ -188,7 +190,7 @@
     copy.wait()
     inv = lax.rsqrt((sq + sq_other[:, 0:1]) / D + epsilon)
     inv_out[...] = jnp.broadcast_to(inv, (TOK, 128))
-    normed[...] = (m32 * inv * gain[...].astype(F32)).astype(BF16)
+    normed[...] = (m32 * inv * gain[...].astype(F32).reshape(1, HALF)).astype(BF16)
 
     def part_at(buf, lead, depth, k):
         if depth == 0:
@@ -199,7 +201,7 @@
 
     def hop(stage, j):
         src, lead, dst = (
-            (s0, j % 6, r1),
+            (s0, j, r1),
             (r1, j, r2),
             (r2, j, r3),
             (t0, (j + 2) % RING, t1),
@@ -216,7 +218,7 @@
                 pltpu.make_async_remote_copy(
                     part_at(src, lead, depth, there),
                     dst.at[j, me],
-                    send.at[stage, j % 6, off - 1],
+                    send.at[stage, j, off - 1],
                     recv.at[stage, j, off - 1],
                     device_id=device,
                     device_id_type=MESH,
@@ -224,7 +226,7 @@
             )
         copies.append(
             pltpu.make_async_copy(
-                part_at(src, lead, depth, me), dst.at[j, me], local.at[stage, j % 6]
+                part_at(src, lead, depth, me), dst.at[j, me], local.at[stage, j]
             )
         )
         return copies
@@ -239,8 +241,8 @@
 
     def pair(kind, j):
         src, dst = (
-            (tok_o.at[(j + 2) % RING], tok_p.at[j]),
-            (cot_o.at[(j + 2) % RING], cot_p.at[j]),
+            (tok_o.at[(j + 2) % 6], tok_p.at[j]),
+            (cot_o.at[(j + 2) % 6], cot_p.at[j]),
             (theirs.at[(j + 2) % RING], got.at[j]),
         )[kind]
         return pltpu.make_async_remote_copy(
@@ -256,9 +258,9 @@
         rows = pl.ds(pl.multiple_of(j * 128, 128), 128)
         k = (j + 2) % RING
         pairs = (
-            (tok_o.at[k], tok_out.at[rows, own_cols]),
+            (tok_o.at[(j + 2) % 6], tok_out.at[rows, own_cols]),
             (tok_p.at[j], tok_out.at[rows, oth_cols]),
-            (cot_o.at[k], cot_out.at[rows, own_cols]),
+            (cot_o.at[(j + 2) % 6], cot_out.at[rows, own_cols]),
             (cot_p.at[j], cot_out.at[rows, oth_cols]),
             (hid.at[k], hid_out.at[rows]),
             (dg.at[k], dg_out.at[rows]),
@@ -284,7 +286,7 @@
             stack = jnp.concatenate(
                 [v[rows, p * 256 : (p + 1) * 256] for v in (a, b) for p in range(4)], axis=0
             )
-            s0[j % 6, n] = mm(mix[...], stack).astype(BF16).reshape(4, 4, 16, 256)
+            s0[j, n] = mm(mix[...], stack).astype(BF16).reshape(4, 4, 16, 256)
         launch(0, j)
 
     def settle(j):
@@ -292,8 +294,7 @@
             cp.wait()
 
     def unpack(j):
-        k = (j + 2) % RING
-        pl.when(j >= RING)(lambda: settle(j - RING))
+        k = (j + 2) % 6
         for n in range(4):
             rows = slice(n * 32, n * 32 + 32)
             v = mm(unmix[...], r3[j, n].reshape(256, 256)).astype(BF16)
@@ -304,11 +305,11 @@
         pair(0, j).start()
         pair(1, j).start()
 
-    def work(j0, n):
+    def work(j0, n, held):
         m = n * 128
         ring = pl.ds(2 if n == 1 else 0, n)
         jobs = pl.ds(j0, n)
-        xo, yo = tok_o[ring].reshape(m, HALF), cot_o[ring].reshape(m, HALF)
+        xo, yo = tok_o[held].reshape(m, HALF), cot_o[held].reshape(m, HALF)
         pre_g = mm(xo, wg[own_cols, :])
         pre_u = mm(xo, wu[own_cols, :])
         d_h = mm_nt(yo, wd[:, own_cols])
@@ -382,26 +383,31 @@
 
         lax.fori_loop(0, 3, one, 0)
 
-    def step(t, carry):
-        trio(t - 5, relay(4))
-        trio(t - 4, relay(3))
-        trio(t - 2, relay(1))
-        trio(t - 1, relay(0))
-        trio(t + 1, select)
-        trio(t - 3, arrive)
-        pl.when(t == 3)(lambda: work(0, 1))
-        pl.when((t > 3) & (t < 7))(lambda: work(3 * t - 11, 3))
-        trio(t - 6, finish)
-        trio(t - 3, give_back)
+    def each(fn):
+        def one(j, carry):
+            fn(j)
+            return carry
+
+        lax.fori_loop(0, JOBS, one, 0)
+
+    def step(g, carry):
+        trio(g - 1, settle)
+        pl.when(g == 0)(lambda: work(0, 1, pl.ds(2, 1)))
+        pl.when((g > 0) & (g < 4))(lambda: work(3 * g - 2, 3, pl.ds(3 * (g % 2), 3)))
+        trio(g - 2, relay(4))
+        trio(g - 1, relay(3))
+        trio(g + 1, arrive)
+        trio(g - 3, finish)
+        trio(g, give_back)
         return carry
 
-    select(0)
-    trio(1, select)
+    each(select)
+    each(relay(0))
+    each(relay(1))
     for cp in loads:
         cp.wait()
-    lax.fori_loop(1, 10, step, 0)
-    for j in range(JOBS - RING, JOBS):
-        settle(j)
+    arrive(0)
+    lax.fori_loop(0, 7, step, 0)
 
 
 def moe(mid, cot, gain, ids_t, prob, share, wg, wu, wd):
@@ -428,12 +434,12 @@
             pltpu.VMEM((8, TOK), F32),
             pltpu.VMEM((256, 256), BF16),
             pltpu.VMEM((256, 256), BF16),
-            pltpu.VMEM((6, 4, 4, 4, 16, 256), BF16),
             pltpu.VMEM((JOBS, 4, 4, 4, 16, 256), BF16),
             pltpu.VMEM((JOBS, 4, 4, 4, 16, 256), BF16),
             pltpu.VMEM((JOBS, 4, 4, 4, 16, 256), BF16),
-            pltpu.VMEM((RING, 128, HALF), BF16),
-            pltpu.VMEM((RING, 128, HALF), BF16),
+            pltpu.VMEM((JOBS, 4, 4, 4, 16, 256), BF16),
+            pltpu.VMEM((6, 128, HALF), BF16),
+            pltpu.VMEM((6, 128, HALF), BF16),
             pltpu.VMEM((JOBS, 128, HALF), BF16),
             pltpu.VMEM((JOBS, 128, HALF), BF16),
             pltpu.VMEM((RING, 128, FF), BF16),
@@ -451,9 +457,9 @@
             pltpu.VMEM((D, FF), BF16),
             pltpu.VMEM((FF, D), BF16),
             pltpu.SemaphoreType.DMA((2,)),
-            pltpu.SemaphoreType.DMA((6, 6, 3)),
             pltpu.SemaphoreType.DMA((6, JOBS, 3)),
-            pltpu.SemaphoreType.DMA((6, 6)),
+            pltpu.SemaphoreType.DMA((6, JOBS, 3)),
+            pltpu.SemaphoreType.DMA((6, JOBS)),
             pltpu.SemaphoreType.DMA((3, RING)),
             pltpu.SemaphoreType.DMA((3, JOBS)),
             pltpu.SemaphoreType.DMA((7, RING)),
@@ -493,7 +499,7 @@
     own_rows = pl.ds(pl.multiple_of(tp * HALF, HALF), HALF)
     oth_rows = pl.ds(pl.multiple_of((1 - tp) * HALF, HALF), HALF)
     greet(other)
-    g_dn = dn[...] * gain[...].astype(F32)
+    g_dn = dn[...] * gain[...].astype(F32).reshape(1, HALF)
     m32 = mid[...].astype(F32)
     inner = jnp.sum(m32 * g_dn, axis=1, keepdims=True)
     in_mine[...] = jnp.broadcast_to(inner, (TOK, 128))
@@ -503,7 +509,7 @@
     copy.start()
     b32 = bg[...].astype(F32)
     y32 = co[...].astype(F32)
-    cg = cgain[...].astype(F32)
+    cg = cgain[...].astype(F32).reshape(1, 512)
     gated = b32 * y32
     same = ind(iota((512, 512), 0) // GROUP == iota((512, 512), 1) // GROUP)
 
@@ -560,7 +566,7 @@
             pltpu.SemaphoreType.DMA((2,)),
         ],
         compiler_params=pltpu.CompilerParams(
-            collective_id=2, has_side_effects=True, vmem_limit_bytes=40 * 2**20
+            collective_id=2, has_side_effects=True, vmem_limit_bytes=62 * 2**20
         ),
         cost_estimate=pl.CostEstimate(
             flops=5 * 10**9, bytes_accessed=12 * 10**6, transcendentals=0
@@ -598,14 +604,14 @@
     conv_out,
     conv_taps,
 ):
-    gain = ffn_gain.reshape(1, HALF)
+    gain = ffn_gain
     d_normed, inv, tok, cot, hid, dg, du = moe(
         mid_stream,
         layer_cot,
         gain,
         expert_ids.T,
-        group_prob.reshape(1, TOK),
-        first_share.reshape(1, TOK),
+        group_prob,
+        first_share,
         expert_gate[0],
         expert_up[0],
         expert_down[0],
@@ -621,7 +627,7 @@
         inv,
         b_gate,
         conv_out,
-        conv_gain.reshape(1, 512),
+        conv_gain,
         out_weight,
     )
     parts = lax.all_to_all(gow.reshape(NDEV, 32, 512), "sp", 0, 0, tiled=True)

time: 186 us -> 170 us (0.914)
  local copies, waits for them, and re-layouts: 10.9 us -> 1.67 us
  Pallas kernels: 134 us -> 130 us
    pallas_call x1, Pallas kernels: 128 us -> 120 us  [moe(): pl.pallas_call(moe_kernel, name='moe', out_shape=(jax.ShapeDtypeStruct((T...]
    unnamed x35 -> x23, local copies, waits for them, and re-layouts: 6.45 us -> 1.65 us
    reshape x4 -> x0, local copies, waits for them, and re-layouts: 4.45 us -> none  [the longest x1 1.28 us: shards(): gain = ffn_gain.reshape(1, HALF)]
    pallas_call x1, Pallas kernels: 6.19 us -> 9.81 us  [tail(): pl.pallas_call(tail_kernel, name='tail', out_shape=(jax.ShapeDtypeStruct(...]
  transfers between devices with their start and end apart: 2 -> 2, of which waited for: 2 -> 2; matrix products, arithmetic and copies ran while one was open for 11% -> 13% of each run, Pallas kernels for 0% -> 0%
where the time goes in v3:
time: 170 us
  Pallas kernels  130 us (76%)
  matrix products  19.6 us (12%)
  waiting for transfers between devices  7.84 us (5%)
  starting transfers between devices  7.37 us (4%)
  other arithmetic  2.76 us (2%)
    pallas_call x1, Pallas kernels, moe(): pl.pallas_call(moe_kernel, name='moe', out_shape=(jax.ShapeDtypeStruct((T...  120 us
    dot_general x3, matrix products, contract_rows(): lax.dot_general(left, right, (((0,), (0,)), ((), ())), preferred_element_...  19.6 us
    pallas_call x1, Pallas kernels, tail(): pl.pallas_call(tail_kernel, name='tail', out_shape=(jax.ShapeDtypeStruct(...  9.81 us
    all_to_all x1, starting transfers between devices, shards(): parts = lax.all_to_all(gow.reshape(NDEV, 32, 512), 'sp', 0, 0, tiled=True)  6.08 us
    all_to_all x1, waiting for transfers between devices, shards(): parts = lax.all_to_all(gow.reshape(NDEV, 32, 512), 'sp', 0, 0, tiled=True)  4.25 us
    ppermute x1, waiting for transfers between devices, from_behind(): return lax.ppermute(block, axis, route)  3.6 us
  transfers between devices with their start and end apart: 2, of which 2 were waited for; matrix products, arithmetic and copies ran while one was open for 13% of the time, Pallas kernels for 0%

profile of v3, /device:TPU:0, one launch (start us, length us, event | category | flops | bytes accessed | tf_op | source)
XLA Modules:
  0.0 169.8 jit_solution(1365538140964968212)
XLA Ops:
  0.6 120.0 %moe.1 = (f32[320,1024]{1,0:T(8,128)}, f32[320,128]{1,0:T(8,128)}, bf16[1280,2048]{1,0:T(8,128)(2,1)}, bf16[1280,2048]{1,0:T(8,128)(2,1)}, bf16[1280,512]{1,0:T(...) custom-call(bf16[320,1024]{1,0:T(8,128)(2,1)} %mid.3, bf16[320,1024]{1,0:T(8,128)(2,1)} %cot.3, ...), custom_call_target="tpu_custom_call" | custom-call | flops 20000000000 | bytes 30000000 | tf_op jit(solution)/shard_map/moe/pallas_call | solution.py:414
  120.6 9.8 %tail.1 = (bf16[2048,512]{1,0:T(8,128)(2,1)}, bf16[320,1024]{1,0:T(8,128)(2,1)}, bf16[320,512]{1,0:T(8,128)(2,1)}, f32[320,512]{1,0:T(8,128)}) custom-call(f32[320,1024]{1,0:T(8,128)} %get-tuple-element.24.dn, bf16[320,1024]{1,0:T(8,128)(2,1)} %mid.3, bf16[320,1024]{1,0:T(8,128)(2,1)} %cot.3, bf16[1024]{0:T(1024)(128)(2,1)} %gain.3, ...), custom_call_target="tpu_custom_call" | custom-call | flops 5000000000 | bytes 12000000 | tf_op jit(solution)/shard_map/tail/pallas_call | solution.py:550
  130.5 0.0 copy-start
  130.5 0.0 copy-start.6
  130.5 6.1 %all-to-all-start = ((bf16[64,32,512]{2,1,0:T(8,128)(2,1)}), bf16[64,32,512]{2,1,0:T(8,128)(2,1)S(1)}, u32[]{:S(2)}, u32[]{:S(2)}) async-start(bf16[64,32,512]{2,1,0:T(8,128)(2,1)} %bitcast.22), calls=%async_computation | async-start | bytes 4194304 | tf_op jit(solution)/shard_map/all_to_all | solution.py:633
  136.6 0.0 copy-done
  136.6 1.3 collective-permute-start
  137.9 0.0 copy-done.6
  137.9 0.0 copy-start.7
  137.9 0.0 slice-start
  137.9 8.0 %convolution_bitcast_fusion.2 = f32[1,2048,512]{2,1,0:T(8,128)} fusion(bf16[1280,2048]{1,0:T(8,128)(2,1)} %get-tuple-element.19, bf16[1280,512]{1,0:T(8,128)(2,1)} %get-tuple-element.20), kind=kOutput, calls=%fused_computation.3 | convolution fusion | flops 2684354560 | bytes 10747904 | tf_op jit(solution)/shard_map/dot_general | solution.py:584
  145.9 0.0 copy-done.7
  145.9 0.0 slice-start.1
  145.9 0.0 copy-start.1
  145.9 7.2 %convolution_bitcast_fusion.1 = f32[1,2048,512]{2,1,0:T(8,128)} fusion(bf16[1280,2048]{1,0:T(8,128)(2,1)} %get-tuple-element.19, bf16[1280,512]{1,0:T(8,128)(2,1)S(1)} %copy-done.7), kind=kOutput, calls=%fused_computation.2 | convolution fusion | flops 2684354560 | bytes 10747904 | tf_op jit(solution)/shard_map/dot_general | solution.py:584
  153.1 0.0 slice-done
  153.1 0.0 slice-done.1
  153.1 0.0 copy-done.1
  153.1 0.0 copy-start.5
  153.1 4.4 %convolution_bitcast_fusion = f32[1,512,2048]{2,1,0:T(8,128)} fusion(bf16[1280,512]{1,0:T(8,128)(2,1)S(1)} %copy-done.1, bf16[1280,2048]{1,0:T(8,128)(2,1)S(1)} %bitcast.21), kind=kOutput, calls=%fused_computation.1 | convolution fusion | flops 2684354560 | bytes 10747904 | tf_op jit(solution)/shard_map/dot_general | solution.py:584
  157.5 0.0 copy-start.3
  157.6 3.6 %collective-permute-done = f32[2,512]{1,0:T(2,128)S(1)} collective-permute-done((f32[2,512]{1,0:T(2,128)S(1)}, f32[2,512]{1,0:T(2,128)S(1)}, u32[]{:S(2)}, u32[]{:S(2)}) %collective-permute-start) | collective-permute-done | bytes 4128 | tf_op jit(solution)/shard_map/ppermute | solution.py:580
  161.2 0.0 copy-done.5
  161.2 1.0 multiply_convert_fusion
  162.2 0.0 copy-start.2
  162.2 0.0 copy-done.3
  162.2 0.0 copy-start.4
  162.2 0.8 multiply_convert_fusion.1
  163.0 4.2 %all-to-all-done = bf16[64,32,512]{2,1,0:T(8,128)(2,1)S(1)} async-done(((bf16[64,32,512]{2,1,0:T(8,128)(2,1)}), bf16[64,32,512]{2,1,0:T(8,128)(2,1)S(1)}, u32[]{:S(2)}, u32[]{:S(2)}) %all-to-all-start) | async-done | bytes 2097184 | tf_op jit(solution)/shard_map/all_to_all | solution.py:633
  167.3 0.9 convert_reduce_fusion
  168.2 0.0 copy-done.2
  168.2 0.8 copy.27
  169.1 0.0 copy-done.4
  169.1 0.7 copy.28
  (5 shorter events, 0.1 us)
Async XLA Ops:
  130.5 6.1 %copy-start = (f32[320,512]{1,0:T(8,128)S(1)}, f32[320,512]{1,0:T(8,128)}, u32[]{:S(2)}) copy-start(f32[320,512]{1,0:T(8,128)} %get-tuple-element.29) | copy-start | bytes 1966084
  130.5 7.4 %copy-start.6 = (bf16[3,512]{1,0:T(4,128)(2,1)S(1)}, bf16[3,512]{1,0:T(4,128)(2,1)}, u32[]{:S(2)}) copy-start(bf16[3,512]{1,0:T(4,128)(2,1)} %param.31) | copy-start | bytes 9220
  130.5 36.8 %all-to-all-start = ((bf16[64,32,512]{2,1,0:T(8,128)(2,1)}), bf16[64,32,512]{2,1,0:T(8,128)(2,1)S(1)}, u32[]{:S(2)}, u32[]{:S(2)}) async-start(bf16[64,32,512]{2,1,0:T(8,128)(2,1)} %bitcast.22), calls=%async_computation | async-start | bytes 4194304 | tf_op jit(solution)/shard_map/all_to_all | solution.py:633
  136.6 24.6 %collective-permute-start = (f32[2,512]{1,0:T(2,128)S(1)}, f32[2,512]{1,0:T(2,128)S(1)}, u32[]{:S(2)}, u32[]{:S(2)}) collective-permute-start(f32[2,512]{1,0:T(2,128)S(1)} %slice.20), channel_id=1, source_target_pairs={{2,0},{4,2},{6,4},{8,6},{10,8},{12,10},{14,12},{16,14},{18,16},{20... | collective-permute-start | bytes 12296 | tf_op jit(solution)/shard_map/ppermute | solution.py:580
  137.9 8.0 %copy-start.7 = (bf16[1280,512]{1,0:T(8,128)(2,1)S(1)}, bf16[1280,512]{1,0:T(8,128)(2,1)}, u32[]{:S(2)}) copy-start(bf16[1280,512]{1,0:T(8,128)(2,1)} %get-tuple-element.21) | copy-start | bytes 3932164
  137.9 15.1 %slice-start = ((s8[5242880]{0:T(1024)(128)(4,1)}), s8[4194304]{0:T(1024)(128)(4,1)S(1)}, s32[]{:S(2)}) async-start(s8[5242880]{0:T(1024)(128)(4,1)} %bitcast.20), calls=%async_computation.1 | async-start | bytes 8388608
  145.9 7.2 %slice-start.1 = ((s8[5242880]{0:T(1024)(128)(4,1)}), s8[1048576]{0:T(1024)(128)(4,1)S(1)}, s32[]{:S(2)}) async-start(s8[5242880]{0:T(1024)(128)(4,1)} %bitcast.20), calls=%async_computation.2 | async-start | bytes 2097152
  145.9 7.2 %copy-start.1 = (bf16[1280,512]{1,0:T(8,128)(2,1)S(1)}, bf16[1280,512]{1,0:T(8,128)(2,1)}, u32[]{:S(2)}) copy-start(bf16[1280,512]{1,0:T(8,128)(2,1)} %get-tuple-element.22) | copy-start | bytes 3932164
  153.1 8.1 %copy-start.5 = (bf16[320,512]{1,0:T(8,128)(2,1)S(1)}, bf16[320,512]{1,0:T(8,128)(2,1)}, u32[]{:S(2)}) copy-start(bf16[320,512]{1,0:T(8,128)(2,1)} %param.28) | copy-start | bytes 983044
  157.5 4.6 %copy-start.3 = (bf16[320,512]{1,0:T(8,128)(2,1)S(1)}, bf16[320,512]{1,0:T(8,128)(2,1)}, u32[]{:S(2)}) copy-start(bf16[320,512]{1,0:T(8,128)(2,1)} %param.29) | copy-start | bytes 983044
  162.2 6.0 %copy-start.2 = (bf16[320,1024]{1,0:T(8,128)(2,1)S(1)}, bf16[320,1024]{1,0:T(8,128)(2,1)}, u32[]{:S(2)}) copy-start(bf16[320,1024]{1,0:T(8,128)(2,1)} %get-tuple-element.47) | copy-start | bytes 1966084
  162.2 6.9 %copy-start.4 = (bf16[320,512]{1,0:T(8,128)(2,1)S(1)}, bf16[320,512]{1,0:T(8,128)(2,1)}, u32[]{:S(2)}) copy-start(bf16[320,512]{1,0:T(8,128)(2,1)} %get-tuple-element.48) | copy-start | bytes 983044

commit v4 on v3

--- a/solution.py
+++ b/solution.py
@@ -93,8 +93,14 @@
     wg_in,
     wu_in,
     wd_in,
-    dn,
-    inv_out,
+    bg,
+    co,
+    cgain,
+    ow_in,
+    gow_out,
+    mgrad,
+    gb,
+    dco,
     tok_out,
     cot_out,
     hid_out,
@@ -138,6 +144,13 @@
     precv,
     osem,
     wsem,
+    dn,
+    inv_out,
+    in_other,
+    rms_s,
+    cn_s,
+    tsend,
+    trecv,
 ):
     sp, tp = lax.axis_index("sp"), lax.axis_index("tp")
     other = (sp, 1 - tp)
@@ -201,7 +214,7 @@
 
     def hop(stage, j):
         src, lead, dst = (
-            (s0, j, r1),
+            (s0, j % 7, r1),
             (r1, j, r2),
             (r2, j, r3),
             (t0, (j + 2) % RING, t1),
@@ -243,7 +256,7 @@
         src, dst = (
             (tok_o.at[(j + 2) % 6], tok_p.at[j]),
             (cot_o.at[(j + 2) % 6], cot_p.at[j]),
-            (theirs.at[(j + 2) % RING], got.at[j]),
+            (theirs.at[(j + 2) % RING], got.at[(j + 2) % 6]),
         )[kind]
         return pltpu.make_async_remote_copy(
             src,
@@ -286,7 +299,7 @@
             stack = jnp.concatenate(
                 [v[rows, p * 256 : (p + 1) * 256] for v in (a, b) for p in range(4)], axis=0
             )
-            s0[j, n] = mm(mix[...], stack).astype(BF16).reshape(4, 4, 16, 256)
+            s0[j % 7, n] = mm(mix[...], stack).astype(BF16).reshape(4, 4, 16, 256)
         launch(0, j)
 
     def settle(j):
@@ -304,6 +317,12 @@
                 cot_o[k, rows, cols] = v[128 + p * 32 : 128 + (p + 1) * 32]
         pair(0, j).start()
         pair(1, j).start()
+
+    def back_rows(buf, ring, g, u, half, n):
+        for h in range(2):
+            w = pl.ds(pl.multiple_of(half * HALF + h * 512, 512), 512)
+            back = mm_nt(g, wg[w, :]) + mm_nt(u, wu[w, :])
+            buf[ring, :, h * 512 : (h + 1) * 512] = back.astype(BF16).reshape(n, 128, 512)
 
     def work(j0, n, held):
         m = n * 128
@@ -328,12 +347,10 @@
         u = (d_h * active).astype(BF16)
         dg[ring] = g.reshape(n, 128, FF)
         du[ring] = u.reshape(n, 128, FF)
-        back = mm_nt(g, wg[oth_cols, :]) + mm_nt(u, wu[oth_cols, :])
-        theirs[ring] = back.astype(BF16).reshape(n, 128, HALF)
+        back_rows(theirs, ring, g, u, 1 - tp, n)
         for d in range(n):
             pair(2, j0 + d).start()
-        back = mm_nt(g, wg[own_cols, :]) + mm_nt(u, wu[own_cols, :])
-        mine[ring] = back.astype(BF16).reshape(n, 128, HALF)
+        back_rows(mine, ring, g, u, tp, n)
         for d in range(n):
             for cp in keep(j0 + d):
                 cp.start()
@@ -341,7 +358,7 @@
     def give_back(j):
         k = (j + 2) % RING
         pair(2, j).wait()
-        s = (mine[k].astype(F32) + got[j].astype(F32)).astype(BF16)
+        s = (mine[k].astype(F32) + got[(j + 2) % 6].astype(F32)).astype(BF16)
         for n in range(4):
             rows = slice(n * 32, n * 32 + 32)
             stack = jnp.concatenate(
@@ -383,12 +400,33 @@
 
         lax.fori_loop(0, 3, one, 0)
 
-    def each(fn):
+    def each(fn, lo, hi):
         def one(j, carry):
             fn(j)
             return carry
 
-        lax.fori_loop(0, JOBS, one, 0)
+        lax.fori_loop(lo, hi, one, 0)
+
+    weigh = pltpu.make_async_copy(ow_in, wu, wsem.at[0])
+
+    def group_mean(v):
+        hi = v.astype(BF16)
+        rest = v - hi.astype(F32)
+        md = rest.astype(BF16)
+        lo = (rest - md.astype(F32)).astype(BF16)
+        ones = ind(iota((512, 512), 0) // GROUP == iota((512, 512), 1) // GROUP).astype(BF16)
+        return (mm(hi, ones) + mm(md, ones) + mm(lo, ones)) / GROUP
+
+    def conv_stats():
+        gated = bg[...].astype(F32) * co[...].astype(F32)
+        rms = lax.rsqrt(group_mean(gated * gated) + epsilon)
+        rms_s[...] = rms
+        cn_s[...] = (gated * rms * cgain[...].astype(F32).reshape(1, 512)).astype(BF16)
+
+    def catch_up():
+        each(relay(1), 4, 7)
+        trio(1, give_back)
+        each(relay(1), 7, JOBS)
 
     def step(g, carry):
         trio(g - 1, settle)
@@ -396,35 +434,79 @@
         pl.when((g > 0) & (g < 4))(lambda: work(3 * g - 2, 3, pl.ds(3 * (g % 2), 3)))
         trio(g - 2, relay(4))
         trio(g - 1, relay(3))
+        pl.when(g == 1)(catch_up)
         trio(g + 1, arrive)
         trio(g - 3, finish)
-        trio(g, give_back)
+        pl.when(g == 4)(lambda: weigh.start())
+        pl.when(g == 5)(conv_stats)
+        pl.when(g != 1)(lambda: trio(g, give_back))
         return carry
 
-    each(select)
-    each(relay(0))
-    each(relay(1))
+    each(select, 0, 7)
+    each(relay(0), 0, 4)
+    each(select, 7, JOBS)
+    each(relay(1), 0, 4)
+    each(relay(0), 4, JOBS)
     for cp in loads:
         cp.wait()
     arrive(0)
     lax.fori_loop(0, 7, step, 0)
-
-
-def moe(mid, cot, gain, ids_t, prob, share, wg, wu, wd):
+    g_dn = dn[...] * gain[...].astype(F32).reshape(1, HALF)
+    m32 = mid[...].astype(F32)
+    inner = jnp.sum(m32 * g_dn, axis=1, keepdims=True)
+    sq_mine[...] = jnp.broadcast_to(inner, (TOK, 128))
+    copy = pltpu.make_async_remote_copy(
+        sq_mine, in_other, tsend.at[0], trecv.at[0], device_id=other, device_id_type=MESH
+    )
+    copy.start()
+    weigh.wait()
+    inv = inv_out[:, 0:1]
+    copy.wait()
+    mean = (inner + in_other[:, 0:1]) / D
+    total = cot[...].astype(F32) + inv * g_dn - m32 * (inv * inv * inv * mean)
+    mgb = total.astype(BF16)
+    mgrad[...] = mgb
+    swap = pltpu.make_async_remote_copy(
+        mgrad, normed, tsend.at[1], trecv.at[1], device_id=other, device_id_type=MESH
+    )
+    swap.start()
+    cn = cn_s[...]
+    wg[own_cols, :] = mm_tn(mgb, cn).astype(BF16)
+    d_cn = mm(mgb, wu[own_cols, :])
+    b32 = bg[...].astype(F32)
+    y32 = co[...].astype(F32)
+    gated = b32 * y32
+    rms = rms_s[...]
+    swap.wait()
+    mo = normed[...]
+    wg[oth_cols, :] = mm_tn(mo, cn).astype(BF16)
+    leave = pltpu.make_async_copy(wg, gow_out, wsem.at[1])
+    leave.start()
+    g_dc = cgain[...].astype(F32).reshape(1, 512) * (d_cn + mm(mo, wu[oth_cols, :]))
+    gmean = group_mean(gated * g_dc)
+    d_gated = rms * g_dc - gated * (rms * rms * rms * gmean)
+    gb[...] = (d_gated * y32).astype(BF16)
+    dco[...] = d_gated * b32
+    leave.wait()
+
+
+def moe(*args):
     return pl.pallas_call(
         moe_kernel,
         name="moe",
         out_shape=(
-            jax.ShapeDtypeStruct((TOK, HALF), F32),
-            jax.ShapeDtypeStruct((TOK, 128), F32),
+            jax.ShapeDtypeStruct((D, 512), BF16),
+            jax.ShapeDtypeStruct((TOK, HALF), BF16),
+            jax.ShapeDtypeStruct((TOK, 512), BF16),
+            jax.ShapeDtypeStruct((TOK, 512), F32),
             jax.ShapeDtypeStruct((ROWS, D), BF16),
             jax.ShapeDtypeStruct((ROWS, D), BF16),
             jax.ShapeDtypeStruct((ROWS, FF), BF16),
             jax.ShapeDtypeStruct((ROWS, FF), BF16),
             jax.ShapeDtypeStruct((ROWS, FF), BF16),
         ),
-        in_specs=[VM] * 6 + [ANY] * 3,
-        out_specs=(VM, VM, ANY, ANY, ANY, ANY, ANY),
+        in_specs=[VM] * 6 + [ANY] * 3 + [VM] * 3 + [ANY],
+        out_specs=(ANY, VM, VM, VM, ANY, ANY, ANY, ANY, ANY),
         scratch_shapes=[
             pltpu.VMEM((TOK, 128), F32),
             pltpu.VMEM((TOK, 128), F32),
@@ -434,7 +516,7 @@
             pltpu.VMEM((8, TOK), F32),
             pltpu.VMEM((256, 256), BF16),
             pltpu.VMEM((256, 256), BF16),
-            pltpu.VMEM((JOBS, 4, 4, 4, 16, 256), BF16),
+            pltpu.VMEM((7, 4, 4, 4, 16, 256), BF16),
             pltpu.VMEM((JOBS, 4, 4, 4, 16, 256), BF16),
             pltpu.VMEM((JOBS, 4, 4, 4, 16, 256), BF16),
             pltpu.VMEM((JOBS, 4, 4, 4, 16, 256), BF16),
@@ -447,7 +529,7 @@
             pltpu.VMEM((RING, 128, FF), BF16),
             pltpu.VMEM((RING, 128, HALF), BF16),
             pltpu.VMEM((RING, 128, HALF), BF16),
-            pltpu.VMEM((JOBS, 128, HALF), BF16),
+            pltpu.VMEM((6, 128, HALF), BF16),
             pltpu.VMEM((RING, 4, 4, 4, 16, 128), BF16),
             pltpu.VMEM((JOBS, 4, 4, 4, 16, 128), BF16),
             pltpu.VMEM((JOBS, 4, 4, 4, 16, 128), BF16),
@@ -464,112 +546,19 @@
             pltpu.SemaphoreType.DMA((3, JOBS)),
             pltpu.SemaphoreType.DMA((7, RING)),
             pltpu.SemaphoreType.DMA((3,)),
-        ],
-        compiler_params=pltpu.CompilerParams(
-            collective_id=1, has_side_effects=True, vmem_limit_bytes=62 * 2**20
-        ),
-        cost_estimate=pl.CostEstimate(
-            flops=20 * 10**9, bytes_accessed=30 * 10**6, transcendentals=655360
-        ),
-    )(mid, cot, gain, ids_t, prob, share, wg, wu, wd)
-
-
-def tail_kernel(
-    dn,
-    mid,
-    cot,
-    gain,
-    inv_in,
-    bg,
-    co,
-    cgain,
-    ow,
-    gow,
-    mgrad,
-    gb,
-    dco,
-    in_mine,
-    in_other,
-    mg,
-    send,
-    recv,
-):
-    sp, tp = lax.axis_index("sp"), lax.axis_index("tp")
-    other = (sp, 1 - tp)
-    own_rows = pl.ds(pl.multiple_of(tp * HALF, HALF), HALF)
-    oth_rows = pl.ds(pl.multiple_of((1 - tp) * HALF, HALF), HALF)
-    greet(other)
-    g_dn = dn[...] * gain[...].astype(F32).reshape(1, HALF)
-    m32 = mid[...].astype(F32)
-    inner = jnp.sum(m32 * g_dn, axis=1, keepdims=True)
-    in_mine[...] = jnp.broadcast_to(inner, (TOK, 128))
-    copy = pltpu.make_async_remote_copy(
-        in_mine, in_other, send.at[0], recv.at[0], device_id=other, device_id_type=MESH
-    )
-    copy.start()
-    b32 = bg[...].astype(F32)
-    y32 = co[...].astype(F32)
-    cg = cgain[...].astype(F32).reshape(1, 512)
-    gated = b32 * y32
-    same = ind(iota((512, 512), 0) // GROUP == iota((512, 512), 1) // GROUP)
-
-    def group_mean(v):
-        hi = v.astype(BF16)
-        rest = v - hi.astype(F32)
-        md = rest.astype(BF16)
-        lo = (rest - md.astype(F32)).astype(BF16)
-        ones = same.astype(BF16)
-        return (mm(hi, ones) + mm(md, ones) + mm(lo, ones)) / GROUP
-
-    rms = lax.rsqrt(group_mean(gated * gated) + epsilon)
-    conv_normed = (gated * rms * cg).astype(BF16)
-    copy.wait()
-    inv = inv_in[:, 0:1]
-    mean = (inner + in_other[:, 0:1]) / D
-    total = cot[...].astype(F32) + inv * g_dn - m32 * (inv * inv * inv * mean)
-    mgb = total.astype(BF16)
-    mgrad[...] = mgb
-    mg[tp] = mgb
-    swap = pltpu.make_async_remote_copy(
-        mg.at[tp], mg.at[tp], send.at[1], recv.at[1], device_id=other, device_id_type=MESH
-    )
-    swap.start()
-    gow[own_rows, :] = mm_tn(mgb, conv_normed).astype(BF16)
-    d_cn = mm(mgb, ow[own_rows, :])
-    swap.wait()
-    mo = mg[1 - tp]
-    gow[oth_rows, :] = mm_tn(mo, conv_normed).astype(BF16)
-    g_dc = cg * (d_cn + mm(mo, ow[oth_rows, :]))
-    gmean = group_mean(gated * g_dc)
-    d_gated = rms * g_dc - gated * (rms * rms * rms * gmean)
-    gb[...] = (d_gated * y32).astype(BF16)
-    dco[...] = d_gated * b32
-
-
-def tail(*args):
-    return pl.pallas_call(
-        tail_kernel,
-        name="tail",
-        out_shape=(
-            jax.ShapeDtypeStruct((D, 512), BF16),
-            jax.ShapeDtypeStruct((TOK, HALF), BF16),
-            jax.ShapeDtypeStruct((TOK, 512), BF16),
-            jax.ShapeDtypeStruct((TOK, 512), F32),
-        ),
-        in_specs=[VM] * 9,
-        out_specs=(VM,) * 4,
-        scratch_shapes=[
+            pltpu.VMEM((TOK, HALF), F32),
             pltpu.VMEM((TOK, 128), F32),
             pltpu.VMEM((TOK, 128), F32),
-            pltpu.VMEM((2, TOK, HALF), BF16),
+            pltpu.VMEM((TOK, 512), F32),
+            pltpu.VMEM((TOK, 512), BF16),
             pltpu.SemaphoreType.DMA((2,)),
             pltpu.SemaphoreType.DMA((2,)),
         ],
         compiler_params=pltpu.CompilerParams(
-            collective_id=2, has_side_effects=True, vmem_limit_bytes=62 * 2**20
+            collective_id=1, has_side_effects=True, vmem_limit_bytes=67043328
         ),
         cost_estimate=pl.CostEstimate(
-            flops=5 * 10**9, bytes_accessed=12 * 10**6, transcendentals=0
+            flops=20 * 10**9, bytes_accessed=30 * 10**6, transcendentals=655360
         ),
     )(*args)
 
@@ -604,32 +593,24 @@
     conv_out,
     conv_taps,
 ):
-    gain = ffn_gain
-    d_normed, inv, tok, cot, hid, dg, du = moe(
+    gow, mid_grad, grad_b, d_conv_out, tok, cot, hid, dg, du = moe(
         mid_stream,
         layer_cot,
-        gain,
+        ffn_gain,
         expert_ids.T,
         group_prob,
         first_share,
         expert_gate[0],
         expert_up[0],
         expert_down[0],
-    )
-    grad_gate = contract_rows(tok, dg)[None]
-    grad_up = contract_rows(tok, du)[None]
-    grad_down = contract_rows(hid, cot)[None]
-    gow, mid_grad, grad_b, d_conv_out = tail(
-        d_normed,
-        mid_stream,
-        layer_cot,
-        gain,
-        inv,
         b_gate,
         conv_out,
         conv_gain,
         out_weight,
     )
+    grad_gate = contract_rows(tok, dg)[None]
+    grad_up = contract_rows(tok, du)[None]
+    grad_down = contract_rows(hid, cot)[None]
     parts = lax.all_to_all(gow.reshape(NDEV, 32, 512), "sp", 0, 0, tiled=True)
     grad_out_weight = jnp.sum(parts.astype(jnp.float32), axis=0)
     following = from_behind(d_conv_out[:2], "sp", -1)

time: 170 us -> 166 us (0.976)
  Pallas kernels: 130 us -> 126 us
  matrix products: 19.6 us -> 16.8 us
  waiting for transfers between devices: 7.84 us -> 10.2 us
    pallas_call x2 -> x1, Pallas kernels: 130 us -> 126 us  [moe(): pl.pallas_call(moe_kernel, name='moe', out_shape=(jax.ShapeDtypeStruct((D...]
    dot_general x3, matrix products: 19.6 us -> 16.8 us  [contract_rows(): lax.dot_general(left, right, (((0,), (0,)), ((), ())), preferred_element_...]
    ppermute x1, waiting for transfers between devices: 3.6 us -> 6.09 us  [from_behind(): return lax.ppermute(block, axis, route)]
  transfers between devices with their start and end apart: 2 -> 2, of which waited for: 2 -> 2; matrix products, arithmetic and copies ran while one was open for 13% -> 11% of each run, Pallas kernels for 0% -> 0%
where the time goes in v4:
time: 166 us
  Pallas kernels  126 us (76%)
  matrix products  16.8 us (10%)
  waiting for transfers between devices  10.2 us (6%)
  starting transfers between devices  7.61 us (5%)
  other arithmetic  2.76 us (2%)
  local copies, waits for them, and re-layouts  1.67 us (1%)
    pallas_call x1, Pallas kernels, moe(): pl.pallas_call(moe_kernel, name='moe', out_shape=(jax.ShapeDtypeStruct((D...  126 us
    dot_general x3, matrix products, contract_rows(): lax.dot_general(left, right, (((0,), (0,)), ((), ())), preferred_element_...  16.8 us
    all_to_all x1, starting transfers between devices, shards(): parts = lax.all_to_all(gow.reshape(NDEV, 32, 512), 'sp', 0, 0, tiled=True)  6.31 us
    ppermute x1, waiting for transfers between devices, from_behind(): return lax.ppermute(block, axis, route)  6.09 us
    all_to_all x1, waiting for transfers between devices, shards(): parts = lax.all_to_all(gow.reshape(NDEV, 32, 512), 'sp', 0, 0, tiled=True)  4.14 us
  transfers between devices with their start and end apart: 2, of which 2 were waited for; matrix products, arithmetic and copies ran while one was open for 11% of the time, Pallas kernels for 0%

profile of v4, /device:TPU:0, one launch (start us, length us, event | category | flops | bytes accessed | tf_op | source)
XLA Modules:
  0.0 165.6 jit_solution(4501029622121308755)
XLA Ops:
  0.6 125.7 %moe.1 = (bf16[2048,512]{1,0:T(8,128)(2,1)}, bf16[320,1024]{1,0:T(8,128)(2,1)}, bf16[320,512]{1,0:T(8,128)(2,1)}, f32[320,512]{1,0:T(8,128)}, bf16[1280,2048]{1,...) custom-call(bf16[320,1024]{1,0:T(8,128)(2,1)} %mid.1, ...), custom_call_target="tpu_custom_call" | custom-call | flops 20000000000 | bytes 30000000 | tf_op jit(solution)/shard_map/moe/pallas_call | solution.py:494
  126.4 0.0 copy-start
  126.4 0.0 copy-start.6
  126.4 6.3 %all-to-all-start = ((bf16[64,32,512]{2,1,0:T(8,128)(2,1)}), bf16[64,32,512]{2,1,0:T(8,128)(2,1)S(1)}, u32[]{:S(2)}, u32[]{:S(2)}) async-start(bf16[64,32,512]{2,1,0:T(8,128)(2,1)} %bitcast.22), calls=%async_computation | async-start | bytes 4194304 | tf_op jit(solution)/shard_map/all_to_all | solution.py:614
  132.7 0.0 copy-done
  132.7 1.3 collective-permute-start
  134.0 0.0 copy-done.6
  134.0 0.0 copy-start.7
  134.1 0.0 copy-start.8
  134.1 0.0 slice-start
  134.1 8.0 %convolution_bitcast_fusion.2 = f32[1,2048,512]{2,1,0:T(8,128)} fusion(bf16[1280,2048]{1,0:T(8,128)(2,1)} %get-tuple-element.17, bf16[1280,512]{1,0:T(8,128)(2,1)} %get-tuple-element.18), kind=kOutput, calls=%fused_computation.3 | convolution fusion | flops 2684354560 | bytes 10747904 | tf_op jit(solution)/shard_map/dot_general | solution.py:573
  142.0 0.0 copy-done.7
  142.0 0.0 copy-done.8
  142.0 0.0 slice-start.1
  142.1 0.0 copy-start.1
  142.1 4.5 %convolution_bitcast_fusion.1 = f32[1,2048,512]{2,1,0:T(8,128)} fusion(bf16[1280,2048]{1,0:T(8,128)(2,1)S(1)} %copy-done.7, bf16[1280,512]{1,0:T(8,128)(2,1)S(1)} %copy-done.8), kind=kOutput, calls=%fused_computation.2 | convolution fusion | flops 2684354560 | bytes 10747904 | tf_op jit(solution)/shard_map/dot_general | solution.py:573
  146.5 0.0 slice-done
  146.5 0.0 slice-done.1
  146.5 0.0 copy-done.1
  146.5 0.0 copy-start.5
  146.6 4.4 %convolution_bitcast_fusion = f32[1,512,2048]{2,1,0:T(8,128)} fusion(bf16[1280,512]{1,0:T(8,128)(2,1)S(1)} %copy-done.1, bf16[1280,2048]{1,0:T(8,128)(2,1)S(1)} %bitcast.21), kind=kOutput, calls=%fused_computation.1 | convolution fusion | flops 2684354560 | bytes 10747904 | tf_op jit(solution)/shard_map/dot_general | solution.py:573
  151.0 0.0 copy-start.3
  151.0 6.1 %collective-permute-done = f32[2,512]{1,0:T(2,128)S(1)} collective-permute-done((f32[2,512]{1,0:T(2,128)S(1)}, f32[2,512]{1,0:T(2,128)S(1)}, u32[]{:S(2)}, u32[]{:S(2)}) %collective-permute-start) | collective-permute-done | bytes 4128 | tf_op jit(solution)/shard_map/ppermute | solution.py:569
  157.1 0.0 copy-done.5
  157.1 1.0 multiply_convert_fusion
  158.1 0.0 copy-start.2
  158.1 0.0 copy-done.3
  158.1 0.0 copy-start.4
  158.1 0.8 multiply_convert_fusion.1
  158.9 4.1 %all-to-all-done = bf16[64,32,512]{2,1,0:T(8,128)(2,1)S(1)} async-done(((bf16[64,32,512]{2,1,0:T(8,128)(2,1)}), bf16[64,32,512]{2,1,0:T(8,128)(2,1)S(1)}, u32[]{:S(2)}, u32[]{:S(2)}) %all-to-all-start) | async-done | bytes 2097184 | tf_op jit(solution)/shard_map/all_to_all | solution.py:614
  163.1 0.9 convert_reduce_fusion
  164.0 0.0 copy-done.2
  164.0 0.8 copy.27
  164.9 0.0 copy-done.4
  164.9 0.7 copy.28
  (5 shorter events, 0.1 us)
Async XLA Ops:
  126.4 6.3 %copy-start = (f32[320,512]{1,0:T(8,128)S(1)}, f32[320,512]{1,0:T(8,128)}, u32[]{:S(2)}) copy-start(f32[320,512]{1,0:T(8,128)} %get-tuple-element.25) | copy-start | bytes 1966084
  126.4 7.7 %copy-start.6 = (bf16[3,512]{1,0:T(4,128)(2,1)S(1)}, bf16[3,512]{1,0:T(4,128)(2,1)}, u32[]{:S(2)}) copy-start(bf16[3,512]{1,0:T(4,128)(2,1)} %param.31) | copy-start | bytes 9220
  126.4 36.7 %all-to-all-start = ((bf16[64,32,512]{2,1,0:T(8,128)(2,1)}), bf16[64,32,512]{2,1,0:T(8,128)(2,1)S(1)}, u32[]{:S(2)}, u32[]{:S(2)}) async-start(bf16[64,32,512]{2,1,0:T(8,128)(2,1)} %bitcast.22), calls=%async_computation | async-start | bytes 4194304 | tf_op jit(solution)/shard_map/all_to_all | solution.py:614
  132.7 24.4 %collective-permute-start = (f32[2,512]{1,0:T(2,128)S(1)}, f32[2,512]{1,0:T(2,128)S(1)}, u32[]{:S(2)}, u32[]{:S(2)}) collective-permute-start(f32[2,512]{1,0:T(2,128)S(1)} %slice.20), channel_id=1, source_target_pairs={{2,0},{4,2},{6,4},{8,6},{10,8},{12,10},{14,12},{16,14},{18,16},{20... | collective-permute-start | bytes 12296 | tf_op jit(solution)/shard_map/ppermute | solution.py:569
  134.0 8.0 %copy-start.7 = (bf16[1280,2048]{1,0:T(8,128)(2,1)S(1)}, bf16[1280,2048]{1,0:T(8,128)(2,1)}, u32[]{:S(2)}) copy-start(bf16[1280,2048]{1,0:T(8,128)(2,1)} %get-tuple-element.17) | copy-start | bytes 15728644
  134.1 8.0 %copy-start.8 = (bf16[1280,512]{1,0:T(8,128)(2,1)S(1)}, bf16[1280,512]{1,0:T(8,128)(2,1)}, u32[]{:S(2)}) copy-start(bf16[1280,512]{1,0:T(8,128)(2,1)} %get-tuple-element.19) | copy-start | bytes 3932164
  134.1 12.5 %slice-start = ((s8[5242880]{0:T(1024)(128)(4,1)}), s8[4194304]{0:T(1024)(128)(4,1)S(1)}, s32[]{:S(2)}) async-start(s8[5242880]{0:T(1024)(128)(4,1)} %bitcast.20), calls=%async_computation.1 | async-start | bytes 8388608
  142.0 4.5 %slice-start.1 = ((s8[5242880]{0:T(1024)(128)(4,1)}), s8[1048576]{0:T(1024)(128)(4,1)S(1)}, s32[]{:S(2)}) async-start(s8[5242880]{0:T(1024)(128)(4,1)} %bitcast.20), calls=%async_computation.2 | async-start | bytes 2097152
  142.1 4.5 %copy-start.1 = (bf16[1280,512]{1,0:T(8,128)(2,1)S(1)}, bf16[1280,512]{1,0:T(8,128)(2,1)}, u32[]{:S(2)}) copy-start(bf16[1280,512]{1,0:T(8,128)(2,1)} %get-tuple-element.20) | copy-start | bytes 3932164
  146.5 10.6 %copy-start.5 = (bf16[320,512]{1,0:T(8,128)(2,1)S(1)}, bf16[320,512]{1,0:T(8,128)(2,1)}, u32[]{:S(2)}) copy-start(bf16[320,512]{1,0:T(8,128)(2,1)} %param.28) | copy-start | bytes 983044
  151.0 7.1 %copy-start.3 = (bf16[320,512]{1,0:T(8,128)(2,1)S(1)}, bf16[320,512]{1,0:T(8,128)(2,1)}, u32[]{:S(2)}) copy-start(bf16[320,512]{1,0:T(8,128)(2,1)} %param.29) | copy-start | bytes 983044
  158.1 5.9 %copy-start.2 = (bf16[320,1024]{1,0:T(8,128)(2,1)S(1)}, bf16[320,1024]{1,0:T(8,128)(2,1)}, u32[]{:S(2)}) copy-start(bf16[320,1024]{1,0:T(8,128)(2,1)} %get-tuple-element.43) | copy-start | bytes 1966084
  158.1 6.8 %copy-start.4 = (bf16[320,512]{1,0:T(8,128)(2,1)S(1)}, bf16[320,512]{1,0:T(8,128)(2,1)}, u32[]{:S(2)}) copy-start(bf16[320,512]{1,0:T(8,128)(2,1)} %get-tuple-element.44) | copy-start | bytes 983044
